TPU v7x, 32 devices: a whole 2x2x4 slice. The times are simulated.
32 devices in a mesh: ep: 8 (over z, x), tp: 4 (over y, core).
Axes of the slice: x: 2, y: 2, z: 4, core: 2. Of those that a mesh axis runs over, the one named last changes fastest.
Arguments:
- head_inputs_unfiltered: bfloat16 [1024, 4096], P('ep', 'tp'), may hold values from -6 to 6
- group_write_vectors: bfloat16 [1024, 512], P('ep', 'tp'), may hold values from -6 to 6
- group_read_vectors: bfloat16 [1024, 512], P('ep', 'tp'), may hold values from -6 to 6
- output_gate_inputs: bfloat16 [1024, 4096], P('ep', 'tp'), may hold values from -6 to 6
- step_preactivation: float32 [64, 1024], P('tp', 'ep'), may hold values from -3.2 to 3.6
- extra_decay_logs: float32 [64, 1024], P('tp', 'ep'), may hold values from -0.7 to 0
- head_decay_logs: float32 [64], P('tp'), may hold values from -16 to -2.7
- head_filter_taps: bfloat16 [4, 4096], P(None, 'tp'), may hold values from -3 to 3
- write_filter_taps: bfloat16 [4, 512], P(None, 'tp'), may hold values from -3 to 3
- read_filter_taps: bfloat16 [4, 512], P(None, 'tp'), may hold values from -3 to 3
- grouped_norm_gain: float32 [4096], P('tp'), may hold values from 0.1 to 1.9
- mixer_output_weight: bfloat16 [4096, 2048], P('tp'), may hold values from -0.09375 to 0.09375
- expert_input_rows: bfloat16 [4096, 2048], P(('ep', 'tp')), may hold values from -6 to 6
- expert_norm_gain: float32 [2048], replicated, may hold values from 0.1 to 1.9
- routes: int32 [4096, 2], P(('ep', 'tp')), may hold values from 0 to 7, all different within a row; in each aligned block of 128 rows (0 to 127, 128 to 255, ...) at most 48 rows name the same one
- router_chosen_scores: bfloat16 [4096, 2], P(('ep', 'tp')), may hold values from 0.049804688 to 1
- routed_gate_weight: bfloat16 [8, 2048, 1024], P('ep', None, 'tp'), may hold values from -0.125 to 0.125
- routed_up_weight: bfloat16 [8, 2048, 1024], P('ep', None, 'tp'), may hold values from -0.125 to 0.125
- routed_down_weight: bfloat16 [8, 1024, 2048], P('ep', 'tp'), may hold values from -0.1875 to 0.1875
- shared_gate_weight: bfloat16 [2048, 512], P(None, 'tp'), may hold values from -0.125 to 0.125
- shared_up_weight: bfloat16 [2048, 512], P(None, 'tp'), may hold values from -0.125 to 0.125
- shared_down_weight: bfloat16 [512, 2048], P('tp'), may hold values from -0.25 to 0.25
Outputs:
- mixer_result: bfloat16 [1024, 2048], P(('ep', 'tp'))
- moe_result: bfloat16 [4096, 2048], P(('ep', 'tp'))
Inputs may be any that keep to these rules, and one draw needn't show every extreme that they name: `routes`: within the 128 rows of one device no expert is named more than 48 times; a row names 2 different experts.
All inputs are finite; a program needn't handle non-finite values.
Results may differ from a plain program's by a relative error of at most 0.0095.
Values may be sent and summed in bfloat16 or wider, within the bound.
A program may use at most 128 MiB of HBM per device.

v0:
```python
import jax
import jax.numpy as jnp
from jax import lax
from jax.sharding import PartitionSpec as P

HEAD_DIM = 64
STATE = 128
BLOCK = 64


eps_norm = 1e-06
route_scale = 2.5
highest = lax.Precision.HIGHEST


def from_behind(value, axis, by):
    devices = lax.axis_size(axis)
    pairs = [(i, i + by) for i in range(devices) if 0 <= i + by < devices]
    return lax.ppermute(value, axis, pairs)


def sent_state(decay, state, axis, by):
    heads, width = decay.shape[0], state.shape[-1]
    parts, rest = [], decay
    for _ in range(3):
        part = lax.reduce_precision(rest, exponent_bits=8, mantissa_bits=7)
        parts.append(part)
        rest = rest - part
    decay_rows = jnp.pad(jnp.stack(parts, axis=1), ((0, 0), (0, width - 3)))
    packed = jnp.concatenate([state.reshape(-1, width), decay_rows], axis=0).astype(jnp.bfloat16)
    packed = from_behind(packed, axis, by).astype(jnp.float32)
    return jnp.sum(packed[-heads:, :3], axis=-1), packed[:-heads].reshape(state.shape)


def carried_in(decay, state, axis):
    shape = state.shape
    own = (decay.reshape(-1), state.reshape((-1,) + shape[-2:]))
    before, by = None, 1
    while by < lax.axis_size(axis):
        span = own if before is None else combine_states(before, own)
        received = sent_state(*span, axis, by)
        before = received if before is None else combine_states(received, before)
        by *= 2
    if before is None:
        return jnp.zeros_like(state)
    return before[1].reshape(shape)


def combine_states(earlier_part, later_part):
    return (
        earlier_part[0] + later_part[0],
        later_part[1] + jnp.exp(later_part[0])[..., None, None] * earlier_part[1],
    )


def conv_silu(values, weights):
    taps = weights.shape[0]
    length = values.shape[0] - taps + 1
    running_sum = jnp.zeros((length, values.shape[1]), jnp.float32)
    for offset in range(taps):
        running_sum = running_sum + weights[offset].astype(jnp.float32) * values[
            offset : offset + length
        ].astype(jnp.float32)
    return jax.nn.silu(running_sum)


def tail_rows_from_behind(head_inputs, write_vectors, read_vectors, taps):
    start = head_inputs.shape[0] - taps + 1
    tail_rows = jnp.concatenate([head_inputs[start:], write_vectors[start:], read_vectors[start:]], axis=1)
    return from_behind(tail_rows, "ep", 1)


def mixer_rows(
    earlier,
    head_inputs_unfiltered,
    group_write_vectors,
    group_read_vectors,
    output_gate_inputs,
    step_preactivation,
    extra_decay_logs,
    head_decay_logs,
    head_filter_taps,
    write_filter_taps,
    read_filter_taps,
    grouped_norm_gain,
):
    row_total = head_inputs_unfiltered.shape[0]
    head_chans = head_inputs_unfiltered.shape[1]
    write_chans = group_write_vectors.shape[1]
    padded_heads = jnp.concatenate([earlier[:, :head_chans], head_inputs_unfiltered], axis=0)
    padded_write = jnp.concatenate(
        [earlier[:, head_chans : head_chans + write_chans], group_write_vectors], axis=0
    )
    padded_read = jnp.concatenate(
        [earlier[:, head_chans + write_chans :], group_read_vectors], axis=0
    )
    heads_local = step_preactivation.shape[0]
    groups_local = write_chans // STATE
    per_group = heads_local // groups_local
    block_count = row_total // BLOCK
    head_values = conv_silu(padded_heads, head_filter_taps).reshape(
        block_count, BLOCK, groups_local, per_group, HEAD_DIM
    )
    write_values = conv_silu(padded_write, write_filter_taps).reshape(
        block_count, BLOCK, groups_local, STATE
    )
    read_values = conv_silu(padded_read, read_filter_taps).reshape(
        block_count, BLOCK, groups_local, STATE
    )
    step_length_value = jax.nn.softplus(step_preactivation)
    decay_rate_logs = -jnp.exp(head_decay_logs)[:, None] * step_length_value + extra_decay_logs
    step_blocks = step_length_value.reshape(groups_local, per_group, block_count, BLOCK)
    cumulative = jnp.cumsum(
        decay_rate_logs.reshape(groups_local, per_group, block_count, BLOCK), axis=3
    )
    weighted = head_values * jnp.transpose(step_blocks, (2, 3, 0, 1))[..., None]
    lower_mask = jnp.tril(jnp.ones((BLOCK, BLOCK), bool))
    gap_logs = cumulative[..., :, None] - cumulative[..., None, :]
    within = jnp.exp(jnp.where(lower_mask, gap_logs, -jnp.inf))
    affinity = jnp.einsum("blgn,bsgn->gbls", read_values, write_values, precision=highest)
    local_part = jnp.einsum(
        "gebls,bsgep->blgep", affinity[:, None] * within, weighted, precision=highest
    )
    to_end = jnp.exp(cumulative[..., -1:] - cumulative)
    block_states = jnp.einsum(
        "bsgn,bsgep,gebs->bgepn", write_values, weighted, to_end, precision=highest
    )
    block_decay = cumulative[..., -1]
    running = jnp.cumsum(block_decay, axis=2)
    entering = running - block_decay
    earlier_blocks = jnp.tril(jnp.ones((block_count, block_count), bool), -1)
    block_ratio = entering[..., :, None] - running[..., None, :]
    carry_weights = jnp.exp(jnp.where(earlier_blocks, block_ratio, -jnp.inf))
    inside = jnp.einsum("gebc,cgepn->bgepn", carry_weights, block_states, precision=highest)
    device_decay = running[..., -1]
    device_state = jnp.einsum(
        "gec,cgepn->gepn",
        jnp.exp(device_decay[..., None] - running),
        block_states,
        precision=highest,
    )
    incoming = carried_in(device_decay, device_state, "ep")
    states_in = (
        inside + jnp.exp(jnp.transpose(entering, (2, 0, 1)))[..., None, None] * incoming[None]
    )
    carried_part = (
        jnp.einsum("blgn,bgepn->blgep", read_values, states_in, precision=highest)
        * jnp.transpose(jnp.exp(cumulative), (2, 3, 0, 1))[..., None]
    )
    scan_out = (local_part + carried_part).reshape(row_total, groups_local, per_group * HEAD_DIM)
    gate_values = jax.nn.silu(output_gate_inputs.astype(jnp.float32)).reshape(
        row_total, groups_local, per_group * HEAD_DIM
    )
    gated_rows = scan_out * gate_values
    gated_rows = gated_rows * lax.rsqrt(
        jnp.mean(gated_rows * gated_rows, axis=-1, keepdims=True) + eps_norm
    )
    return (gated_rows.reshape(row_total, head_chans) * grouped_norm_gain).astype(jnp.bfloat16)


def local(
    head_inputs_unfiltered,
    group_write_vectors,
    group_read_vectors,
    output_gate_inputs,
    step_preactivation,
    extra_decay_logs,
    head_decay_logs,
    head_filter_taps,
    write_filter_taps,
    read_filter_taps,
    grouped_norm_gain,
    mixer_output_weight,
    expert_input_rows,
    expert_norm_gain,
    routes,
    router_chosen_scores,
    routed_gate_weight,
    routed_up_weight,
    routed_down_weight,
    shared_gate_weight,
    shared_up_weight,
    shared_down_weight,
):
    earlier = tail_rows_from_behind(
        head_inputs_unfiltered, group_write_vectors, group_read_vectors, head_filter_taps.shape[0]
    )
    tp_count = lax.axis_size("tp")
    ep_count = lax.axis_size("ep")
    tok_local = expert_input_rows.shape[0]
    model_width = expert_input_rows.shape[1]
    top_count = routes.shape[1]
    local_experts = routed_gate_weight.shape[0]
    experts = local_experts * ep_count
    capacity = 3 * tok_local * top_count // (2 * experts)
    rows_float = expert_input_rows.astype(jnp.float32)
    normed = (
        rows_float
        * lax.rsqrt(jnp.mean(rows_float * rows_float, axis=-1, keepdims=True) + eps_norm)
        * expert_norm_gain
    ).astype(jnp.bfloat16)
    score_float = router_chosen_scores.astype(jnp.float32)
    weights = score_float / jnp.sum(score_float, axis=1, keepdims=True) * route_scale
    choice = routes[None, :, :] == jnp.arange(experts, dtype=jnp.int32)[:, None, None]
    named = jnp.any(choice, axis=2)
    weight_of = jnp.sum(jnp.where(choice, weights[None], 0.0), axis=2)
    row_order = jnp.arange(tok_local, dtype=jnp.int32)
    earlier_rows = (row_order[:, None] < row_order[None, :]).astype(jnp.bfloat16)
    rank = jnp.dot(
        named.astype(jnp.bfloat16), earlier_rows, preferred_element_type=jnp.float32
    ).astype(jnp.int32)

    cuts = [0, capacity // 2, capacity] if capacity > 1 else [0, capacity]
    picks, outgoing = [], []
    for low, high in zip(cuts[:-1], cuts[1:]):
        places = jnp.arange(low, high, dtype=jnp.int32)
        picked = named[:, None, :] & (rank[:, None, :] == places[None, :, None])
        picks.append(picked)
        outgoing.append(
            jnp.dot(
                picked.reshape(-1, tok_local).astype(jnp.bfloat16),
                normed,
                preferred_element_type=jnp.float32,
            ).astype(jnp.bfloat16)
        )
    group_rows = lax.all_gather(normed, "tp", axis=0, tiled=True)
    earlier, group_rows, outgoing[0] = lax.optimization_barrier((earlier, group_rows, outgoing[0]))

    arrived = []
    for block in outgoing:
        arrived.append(lax.all_to_all(block, "ep", split_axis=0, concat_axis=0, tiled=True))
    gathered = [lax.all_gather(block, "tp", axis=0) for block in arrived]

    shared_hidden = (
        jax.nn.silu(jnp.dot(group_rows, shared_gate_weight, preferred_element_type=jnp.float32))
        * jnp.dot(group_rows, shared_up_weight, preferred_element_type=jnp.float32)
    ).astype(jnp.bfloat16)
    shared_part = jnp.dot(shared_hidden, shared_down_weight, preferred_element_type=jnp.float32)

    mixer_normed = mixer_rows(
        earlier,
        head_inputs_unfiltered,
        group_write_vectors,
        group_read_vectors,
        output_gate_inputs,
        step_preactivation,
        extra_decay_logs,
        head_decay_logs,
        head_filter_taps,
        write_filter_taps,
        read_filter_taps,
        grouped_norm_gain,
    )

    def expert_rows(block):
        sources = block.reshape(tp_count, ep_count, local_experts, -1, model_width)
        gate_value = jnp.einsum(
            "osecd,edf->osecf", sources, routed_gate_weight, preferred_element_type=jnp.float32
        )
        up_value = jnp.einsum(
            "osecd,edf->osecf", sources, routed_up_weight, preferred_element_type=jnp.float32
        )
        hidden = (jax.nn.silu(gate_value) * up_value).astype(jnp.bfloat16)
        partial_value = jnp.einsum(
            "osecf,efd->osecd", hidden, routed_down_weight, preferred_element_type=jnp.float32
        ).astype(jnp.bfloat16)
        return lax.psum_scatter(
            partial_value.reshape(-1, model_width), "tp", scatter_dimension=0, tiled=True
        )

    own_term = jnp.zeros((tok_local, model_width), jnp.float32)
    for block, picked in zip(gathered, picks):
        returned = lax.all_to_all(
            expert_rows(block), "ep", split_axis=0, concat_axis=0, tiled=True
        )
        mixing = jnp.where(picked, weight_of[:, None, :], 0.0).reshape(-1, tok_local)
        own_term = own_term + jnp.einsum(
            "sr,sd->rd", mixing, returned.astype(jnp.float32), precision=highest
        )
    mix_block = mixer_normed.shape[0] // tp_count
    block_rows = mix_block + tok_local
    mix_term = jnp.dot(
        mixer_normed, mixer_output_weight, preferred_element_type=jnp.float32
    ).astype(jnp.bfloat16).reshape(tp_count, mix_block, model_width)
    moe_term = shared_part.astype(jnp.bfloat16).reshape(tp_count, tok_local, model_width)
    row_sums = lax.psum_scatter(
        jnp.concatenate([mix_term, moe_term], axis=1).reshape(tp_count * block_rows, model_width),
        "tp",
        scatter_dimension=0,
        tiled=True,
    )
    mixer_result = row_sums[:mix_block]
    moe_total = row_sums[mix_block:].astype(jnp.float32) + own_term
    return (mixer_result.astype(jnp.bfloat16), moe_total.astype(jnp.bfloat16))


def solution(mesh):
    in_specs = (
        P("ep", "tp"),
        P("ep", "tp"),
        P("ep", "tp"),
        P("ep", "tp"),
        P("tp", "ep"),
        P("tp", "ep"),
        P("tp"),
        P(None, "tp"),
        P(None, "tp"),
        P(None, "tp"),
        P("tp"),
        P("tp", None),
        P(("ep", "tp"), None),
        P(),
        P(("ep", "tp"), None),
        P(("ep", "tp"), None),
        P("ep", None, "tp"),
        P("ep", None, "tp"),
        P("ep", "tp", None),
        P(None, "tp"),
        P(None, "tp"),
        P("tp", None),
    )
    out_specs = (P(("ep", "tp"), None), P(("ep", "tp"), None))
    return jax.shard_map(local, mesh=mesh, in_specs=in_specs, out_specs=out_specs, check_vma=False)
```

profile of v0, /device:TPU:0, one launch (start us, length us, event | category | flops | bytes accessed | tf_op | source)
XLA Modules:
  0.0 231.7 jit_solution(13960025605064493204)
XLA Ops:
  7.3 1.3 fusion.13
  8.6 2.0 fusion.15
  10.9 0.7 fusion.98
  11.6 0.1 convolution_convert_fusion.6
  11.7 0.1 bitcast_and_fusion
  11.8 1.4 convolution_convert_fusion.3
  13.3 27.3 %all_to_all.36 = bf16[8,24,2048]{2,1,0:T(8,128)(2,1)} all-to-all(bf16[8,24,2048]{2,1,0:T(8,128)(2,1)S(1)} %bitcast.295), channel_id=1, replica_groups=mesh['ep'=8,'tp'=4] {'ep'}, dimensions={0} | all-to-all | bytes 1572864 | tf_op jit(solution)/shard_map/all_to_all | solution.py:231
  40.7 3.3 %collective-permute-start = (bf16[3,1280]{1,0:T(4,128)(2,1)S(1)}, bf16[3,1280]{1,0:T(4,128)(2,1)S(1)}, u32[]{:S(2)}, u32[]{:S(2)}) collective-permute-start(bf16[3,1280]{1,0:T(4,128)(2,1)S(1)} %pad_maximum_fusion.4), channel_id=1, source_target_pairs={{0,4},{4,8},{8,12},{12,16},{16,20},{20,24},{24,28},{1,5},{5,9},{9,... | collective-permute-start | bytes 23048 | tf_op jit(solution)/shard_map/ppermute | solution.py:19
  44.1 0.4 convolution_convert_fusion.4
  44.5 1.0 collective-permute-done
  45.5 23.0 %all_to_all.37 = bf16[8,24,2048]{2,1,0:T(8,128)(2,1)} all-to-all(bf16[8,24,2048]{2,1,0:T(8,128)(2,1)S(1)} %bitcast.294), channel_id=1, replica_groups=mesh['ep'=8,'tp'=4] {'ep'}, dimensions={0} | all-to-all | bytes 1572864 | tf_op jit(solution)/shard_map/all_to_all | solution.py:231
  68.6 4.1 %convolution_bitcast_fusion.6 = f32[4,8,1,24,256]{4,3,1,0,2:T(8,128)} fusion(bf16[4,8,24,2048]{3,2,1,0:T(8,128)(2,1)} %bitcast.319, bf16[1,2048,256]{2,1,0:T(8,128)(2,1)} %param.38), kind=kOutput, calls=%fused_computation.20 | convolution fusion | flops 805306368 | bytes 4980736 | tf_op jit(solution)/shard_map/osecd,edf->osecf/dot_general | solution.py:257
  72.7 7.1 %convolution_convert_fusion = bf16[4,8,24,2048]{3,2,1,0:T(8,128)(2,1)} fusion(bf16[4,8,24,2048]{3,2,1,0:T(8,128)(2,1)} %bitcast.320, bf16[1,256,2048]{2,1,0:T(8,128)(2,1)S(1)} %copy-done, bf16[1,2048,256]{2,1,0:T(8,128)(2,1)S(1)} %copy-done.24, f32[4,8,1,24,256]{4,3,1,0,2:T(8,128)} %convolution_bitcast_fusion.6), kind=kOutput, calls=%fused_computation | convolution fusion | flops 1613365248 | bytes 9175040 | tf_op jit(solution)/shard_map/osecf,efd->osecd/dot_general | solution.py:264
  79.9 0.5 copy-done.27
  80.8 0.5 reduce_window_sum.24
  81.2 0.2 slice_reduce_fusion
  81.7 0.6 iota_compare_fusion.6
  82.4 0.6 bitcast_exponential_fusion
  83.2 0.4 divide_multiply_fusion
  83.6 0.3 reshape.451
  83.8 0.4 copy.69
  84.4 2.1 fusion.24
  86.5 11.9 %all-gather.6.cloned.1.call-done = bf16[4,192,2048]{2,1,0:T(8,128)(2,1)} async-done(((bf16[1,192,2048]{2,1,0:T(8,128)(2,1)}), bf16[4,192,2048]{2,1,0:T(8,128)(2,1)}) %all-gather.6.cloned.1.call-update) | async-done | bytes 3145744 | tf_op jit(solution)/shard_map/all_gather | solution.py:232
  98.4 4.0 %convolution_bitcast_fusion.8 = f32[4,8,1,24,256]{4,3,1,0,2:T(8,128)} fusion(bf16[4,8,24,2048]{3,2,1,0:T(8,128)(2,1)} %bitcast.317, bf16[1,2048,256]{2,1,0:T(8,128)(2,1)} %param.38), kind=kOutput, calls=%fused_computation.22 | convolution fusion | flops 805306368 | bytes 4980736 | tf_op jit(solution)/shard_map/osecd,edf->osecf/dot_general | solution.py:257
  102.5 7.1 %convolution_convert_fusion.1 = bf16[4,8,24,2048]{3,2,1,0:T(8,128)(2,1)} fusion(bf16[4,8,24,2048]{3,2,1,0:T(8,128)(2,1)} %bitcast.318, bf16[1,256,2048]{2,1,0:T(8,128)(2,1)S(1)} %copy-done, bf16[1,2048,256]{2,1,0:T(8,128)(2,1)S(1)} %copy-done.25, f32[4,8,1,24,256]{4,3,1,0,2:T(8,128)} %convolution_bitcast_fusion.8), kind=kOutput, calls=%fused_computation.1 | convolution fusion | flops 1613365248 | bytes 9175040 | tf_op jit(solution)/shard_map/osecf,efd->osecd/dot_general | solution.py:264
  109.6 0.2 reduce-scatter.4.cloned.1.call-start
  109.9 5.6 %fusion.32 = f32[16,1,64,128]{3,1,2,0:T(1,128)S(1)} fusion(f32[16,2,1,1]{1,2,3,0:T(1,128)S(1)} %copy.83, f32[2,16,64,128]{3,2,1,0:T(8,128)} %fusion.24), kind=kOutput, calls=%fused_computation.50 | convolution fusion | flops 3145728 | bytes 1572992 | tf_op jit(solution)/shard_map/gec,cgepn->gepn/dot_general | solution.py:136
  115.6 3.5 %collective-permute-start.1 = (bf16[1040,128]{1,0:T(8,128)(2,1)S(1)}, bf16[1040,128]{1,0:T(8,128)(2,1)S(1)}, u32[]{:S(2)}, u32[]{:S(2)}) collective-permute-start(bf16[1040,128]{1,0:T(8,128)(2,1)S(1)} %fusion.63), channel_id=1, source_target_pairs={{0,4},{4,8},{8,12},{12,16},{16,20},{20,24},{24,28},{1,5},{5,9},{9,... | collective-permute-start | bytes 798728 | tf_op jit(solution)/shard_map/ppermute | solution.py:19
  119.0 0.7 copy.75
  119.7 0.8 copy.89
  120.5 0.7 copy.73
  121.2 3.8 %collective-permute-done.1 = bf16[1040,128]{1,0:T(8,128)(2,1)S(1)} collective-permute-done((bf16[1040,128]{1,0:T(8,128)(2,1)S(1)}, bf16[1040,128]{1,0:T(8,128)(2,1)S(1)}, u32[]{:S(2)}, u32[]{:S(2)}) %collective-permute-start.1) | collective-permute-done | bytes 266272 | tf_op jit(solution)/shard_map/ppermute | solution.py:19
  125.1 0.1 slice_reduce_fusion.2
  125.3 0.8 add_convert_fusion.1
  126.2 5.3 %collective-permute-start.2 = (bf16[1040,128]{1,0:T(8,128)(2,1)S(1)}, bf16[1040,128]{1,0:T(8,128)(2,1)S(1)}, u32[]{:S(2)}, u32[]{:S(2)}) collective-permute-start(bf16[1040,128]{1,0:T(8,128)(2,1)S(1)} %fusion.64), channel_id=1, source_target_pairs={{0,8},{4,12},{8,16},{12,20},{16,24},{20,28},{1,9},{5,13},{9,17},{1... | collective-permute-start | bytes 798728 | tf_op jit(solution)/shard_map/ppermute | solution.py:19
  131.5 3.1 %fusion.120 = f32[512,128]{1,0:T(8,128)} fusion(bf16[512,2048]{1,0:T(8,128)(2,1)} %all-gather.4.cloned.1.call-done, bf16[2048,128]{1,0:T(8,128)(2,1)} %param.41), kind=kOutput, calls=%fused_computation.216 | convolution fusion | flops 268435456 | bytes 2883584 | tf_op jit(solution)/shard_map/dot_general | solution.py:235
  134.6 2.0 collective-permute-done.2
  136.7 0.1 slice_reduce_fusion.1
  136.8 0.6 pad_maximum_fusion.7
  137.4 0.8 copy.92
  138.2 0.7 add_exponential_fusion
  138.9 0.8 add_convert_fusion
  139.8 0.7 fusion.65
  140.6 6.2 %collective-permute-start.3 = (bf16[1040,128]{1,0:T(8,128)(2,1)}, bf16[1040,128]{1,0:T(8,128)(2,1)}, u32[]{:S(2)}, u32[]{:S(2)}) collective-permute-start(bf16[1040,128]{1,0:T(8,128)(2,1)} %fusion.65), channel_id=1, source_target_pairs={{0,16},{4,20},{8,24},{12,28},{1,17},{5,21},{9,25},{13,29},{2,18},{... | collective-permute-start | bytes 798728 | tf_op jit(solution)/shard_map/ppermute | solution.py:19
  146.7 5.7 %convolution_convert_fusion.2 = bf16[512,2048]{1,0:T(8,128)(2,1)} fusion(bf16[128,2048]{1,0:T(8,128)(2,1)} %param.43, f32[512,128]{1,0:T(8,128)} %fusion.120, bf16[512,2048]{1,0:T(8,128)(2,1)} %all-gather.4.cloned.1.call-done, bf16[2048,128]{1,0:T(8,128)(2,1)} %param.42), kind=kOutput, calls=%fused_computation.2 | convolution fusion | flops 538312704 | bytes 5505024 | tf_op jit(solution)/shard_map/dot_general | solution.py:238
  152.5 0.2 fusion.119
  152.7 1.0 slice.163
  153.7 0.2 fusion.52
  153.9 5.6 %fusion.10 = f32[2,16,64,128]{3,0,2,1:T(2,128)S(1)} fusion(f32[2,16,64,128]{3,2,1,0:T(8,128)} %fusion.24, f32[16,64,128]{2,1,0:T(8,128)S(1)} %fusion.52, f32[2,16]{0,1:T(8,128)S(1)} %copy-done.13, pred[2,2]{1,0:T(4,128)(4,1)S(1)} %copy-done.28, f32[16,2]{1,0:T(8,128)S(1)} %copy-done.14, f32[16,2]{1,0:T(8,128)S(1)} %bitcast.316), kind=kOutput, calls=%fused_computation.28 | convolution fusion | flops 6815872 | bytes 2621828 | tf_op jit(solution)/shard_map/gebc,cgepn->bgepn/dot_general | solution.py:134
  159.5 1.0 fusion.4
  160.5 2.0 fusion.3
  162.6 0.5 copy.80
  163.1 0.3 reshape.463
  163.4 0.1 copy-done.8
  163.5 0.2 multiply_reduce_fusion
  163.8 3.2 %convolution_convert_fusion.5 = bf16[128,2048]{1,0:T(8,128)(2,1)S(1)} fusion(bf16[1024,2048]{1,0:T(8,128)(2,1)} %param.33, f32[1024]{0:T(1024)S(1)} %copy-done.26, f32[128]{0:T(128)S(1)} %add_rsqrt_fusion, f32[128,1024]{1,0:T(8,128)S(1)} %reshape.463, bf16[128,1024]{1,0:T(8,128)(2,1)S(1)} %copy-done.8), kind=kOutput, calls=%fused_computation.11 | convolution fusion | flops 538312704 | bytes 5509632 | tf_op jit(solution)/shard_map/dot_general | solution.py:282
  167.0 1.7 pad_maximum_fusion
  168.8 30.0 %all_to_all.38 = bf16[8,24,2048]{2,1,0:T(8,128)(2,1)} all-to-all(bf16[8,24,2048]{2,1,0:T(8,128)(2,1)} %bitcast.301), channel_id=1, replica_groups=mesh['ep'=8,'tp'=4] {'ep'}, dimensions={0} | all-to-all | bytes 1572864 | tf_op jit(solution)/shard_map/all_to_all | solution.py:273
  198.8 3.6 %all-to-all-start.1 = ((bf16[8,24,2048]{2,1,0:T(8,128)(2,1)}), bf16[8,24,2048]{2,1,0:T(8,128)(2,1)S(1)}, u32[]{:S(2)}, u32[]{:S(2)}) async-start(bf16[8,24,2048]{2,1,0:T(8,128)(2,1)} %bitcast.302), calls=%async_computation.3 | async-start | bytes 1572864 | tf_op jit(solution)/shard_map/all_to_all | solution.py:273
  202.5 13.4 %reduce-scatter.4.cloned.1.call-done = bf16[160,2048]{1,0:T(8,128)(2,1)} async-done(((bf16[640,2048]{1,0:T(8,128)(2,1)}), bf16[160,2048]{1,0:T(8,128)(2,1)}) %reduce-scatter.4.cloned.1.call-update) | async-done | bytes 655376 | tf_op jit(solution)/shard_map/reduce_scatter | solution.py:286
  215.9 1.6 slice.164
  217.5 1.8 convolution_bitcast_fusion
  219.3 3.0 %all-to-all-done.1 = bf16[8,24,2048]{2,1,0:T(8,128)(2,1)S(1)} async-done(((bf16[8,24,2048]{2,1,0:T(8,128)(2,1)}), bf16[8,24,2048]{2,1,0:T(8,128)(2,1)S(1)}, u32[]{:S(2)}, u32[]{:S(2)}) %all-to-all-start.1) | async-done | bytes 786464 | tf_op jit(solution)/shard_map/all_to_all | solution.py:273
  222.3 2.5 %fusion.2 = bf16[128,2048]{1,0:T(8,128)(2,1)} fusion(f32[128,2048]{1,0:T(8,128)S(1)} %convolution_bitcast_fusion, bf16[8,24,2048]{2,1,0:T(8,128)(2,1)S(1)} %all-to-all-done.1, bf16[160,2048]{1,0:T(8,128)(2,1)} %reduce-scatter.4.cloned.1.call-done, f32[8,128]{1,0:T(8,128)S(1)} %select_reduce_fusion, s32[8,128]{1,0:T(8,128)S(1)} %convolution_convert_fusion.6, ...), kind=kOutput, calls=%fused_computation.10 | convolution fusion | flops 605102080 | bytes 2892800 | tf_op jit(solution)/shard_map/sr,sd->rd/dot_general | solution.py:277
  (124 shorter events, 2.1 us)
Async XLA Ops:
  7.2 65.5 %copy-start = (bf16[1,256,2048]{2,1,0:T(8,128)(2,1)S(1)}, bf16[1,256,2048]{2,1,0:T(8,128)(2,1)}, u32[]{:S(2)}) copy-start(bf16[1,256,2048]{2,1,0:T(8,128)(2,1)} %param.40) | copy-start | bytes 3145732
  7.2 33.5 %copy-start.7 = (bf16[128,1024]{1,0:T(8,128)(2,1)S(1)}, bf16[128,1024]{1,0:T(8,128)(2,1)}, u32[]{:S(2)}) copy-start(bf16[128,1024]{1,0:T(8,128)(2,1)} %param.22) | copy-start | bytes 786436
  7.2 33.5 %copy-start.9 = (bf16[128,128]{1,0:T(8,128)(2,1)S(1)}, bf16[128,128]{1,0:T(8,128)(2,1)}, u32[]{:S(2)}) copy-start(bf16[128,128]{1,0:T(8,128)(2,1)} %param.23) | copy-start | bytes 98308
  7.2 33.5 %copy-start.10 = (bf16[128,128]{1,0:T(8,128)(2,1)S(1)}, bf16[128,128]{1,0:T(8,128)(2,1)}, u32[]{:S(2)}) copy-start(bf16[128,128]{1,0:T(8,128)(2,1)} %param.24) | copy-start | bytes 98308
  7.2 38.2 %all-gather.4.cloned.1.call-start = ((), (), s32[]{:S(2)}) async-start(), calls=%async_computation.7 | async-start | bytes 2621440 | tf_op jit(solution)/shard_map/all_gather | solution.py:226
  10.6 33.5 %copy-start.2 = (bf16[128,2048]{1,0:T(8,128)(2,1)S(1)}, bf16[128,2048]{1,0:T(8,128)(2,1)}, u32[]{:S(2)}) copy-start(bf16[128,2048]{1,0:T(8,128)(2,1)} %fusion.15) | copy-start | bytes 1572868
  10.6 57.9 %all-gather.8.cloned.1.call-start = ((), (), s32[]{:S(2)}) async-start(), calls=%async_computation.11 | async-start | bytes 3932160 | tf_op jit(solution)/shard_map/all_gather | solution.py:232
  10.7 0.9 copy-start.21
  40.6 57.8 %all-gather.6.cloned.1.call-start = ((), (), s32[]{:S(2)}) async-start(), calls=%async_computation.9 | async-start | bytes 3932160 | tf_op jit(solution)/shard_map/all_gather | solution.py:232
  40.7 4.7 %collective-permute-start = (bf16[3,1280]{1,0:T(4,128)(2,1)S(1)}, bf16[3,1280]{1,0:T(4,128)(2,1)S(1)}, u32[]{:S(2)}, u32[]{:S(2)}) collective-permute-start(bf16[3,1280]{1,0:T(4,128)(2,1)S(1)} %pad_maximum_fusion.4), channel_id=1, source_target_pairs={{0,4},{4,8},{8,12},{12,16},{16,20},{20,24},{24,28},{1,5},{5,9},{9,... | collective-permute-start | bytes 23048 | tf_op jit(solution)/shard_map/ppermute | solution.py:19
  68.5 4.2 %copy-start.24 = (bf16[1,2048,256]{2,1,0:T(8,128)(2,1)S(1)}, bf16[1,2048,256]{2,1,0:T(8,128)(2,1)}, u32[]{:S(2)}) copy-start(bf16[1,2048,256]{2,1,0:T(8,128)(2,1)} %param.39) | copy-start | bytes 3145732
  68.5 100.3 %reduce-scatter.8.cloned.1.call-start = ((), (), s32[]{:S(2)}) async-start(), calls=%async_computation.12 | async-start | bytes 3932160 | tf_op jit(solution)/shard_map/reduce_scatter | solution.py:267
  79.8 0.7 copy-start.27
  79.8 0.7 copy-start.15
  79.8 0.7 copy-start.16
  79.8 3.2 %copy-start.18 = (bf16[4,128]{1,0:T(4,128)(2,1)S(1)}, bf16[4,128]{1,0:T(4,128)(2,1)}, u32[]{:S(2)}) copy-start(bf16[4,128]{1,0:T(4,128)(2,1)} %param.30) | copy-start | bytes 3076
  79.8 3.2 %copy-start.19 = (bf16[4,128]{1,0:T(4,128)(2,1)S(1)}, bf16[4,128]{1,0:T(4,128)(2,1)}, u32[]{:S(2)}) copy-start(bf16[4,128]{1,0:T(4,128)(2,1)} %param.31) | copy-start | bytes 3076
  79.8 3.2 %copy-start.11 = (bf16[4,1024]{1,0:T(4,128)(2,1)S(1)}, bf16[4,1024]{1,0:T(4,128)(2,1)}, u32[]{:S(2)}) copy-start(bf16[4,1024]{1,0:T(4,128)(2,1)} %param.29) | copy-start | bytes 24580
  79.8 119.0 %reduce-scatter.6.cloned.1.call-start = ((), (), s32[]{:S(2)}) async-start(), calls=%async_computation.10 | async-start | bytes 3932160 | tf_op jit(solution)/shard_map/reduce_scatter | solution.py:267
  84.4 18.1 %copy-start.5 = (f32[128,128]{1,0:T(8,128)}, f32[128,128]{1,0:T(8,128)S(1)}, u32[]{:S(2)}) copy-start(f32[128,128]{1,0:T(8,128)S(1)} %get-tuple-element.38) | copy-start | bytes 196612
  86.5 16.0 %copy-start.25 = (bf16[1,2048,256]{2,1,0:T(8,128)(2,1)S(1)}, bf16[1,2048,256]{2,1,0:T(8,128)(2,1)}, u32[]{:S(2)}) copy-start(bf16[1,2048,256]{2,1,0:T(8,128)(2,1)} %param.39) | copy-start | bytes 3145732
  109.6 106.3 %reduce-scatter.4.cloned.1.call-start = ((), (), s32[]{:S(2)}) async-start(), calls=%async_computation.8 | async-start | bytes 3276800 | tf_op jit(solution)/shard_map/reduce_scatter | solution.py:286
  115.6 9.5 %collective-permute-start.1 = (bf16[1040,128]{1,0:T(8,128)(2,1)S(1)}, bf16[1040,128]{1,0:T(8,128)(2,1)S(1)}, u32[]{:S(2)}, u32[]{:S(2)}) collective-permute-start(bf16[1040,128]{1,0:T(8,128)(2,1)S(1)} %fusion.63), channel_id=1, source_target_pairs={{0,4},{4,8},{8,12},{12,16},{16,20},{20,24},{24,28},{1,5},{5,9},{9,... | collective-permute-start | bytes 798728 | tf_op jit(solution)/shard_map/ppermute | solution.py:19
  126.2 10.5 %collective-permute-start.2 = (bf16[1040,128]{1,0:T(8,128)(2,1)S(1)}, bf16[1040,128]{1,0:T(8,128)(2,1)S(1)}, u32[]{:S(2)}, u32[]{:S(2)}) collective-permute-start(bf16[1040,128]{1,0:T(8,128)(2,1)S(1)} %fusion.64), channel_id=1, source_target_pairs={{0,8},{4,12},{8,16},{12,20},{16,24},{20,28},{1,9},{5,13},{9,17},{1... | collective-permute-start | bytes 798728 | tf_op jit(solution)/shard_map/ppermute | solution.py:19
  136.8 1.4 copy-start.17
  138.2 1.6 copy-start.3
  139.8 12.7 %copy-start.6 = (f32[128,128]{1,0:T(8,128)S(1)}, f32[128,128]{1,0:T(8,128)}, u32[]{:S(2)}) copy-start(f32[128,128]{1,0:T(8,128)} %copy-done.5) | copy-start | bytes 196612
  140.5 13.1 %copy-start.4 = (f32[1024,128]{1,0:T(8,128)S(1)}, f32[1024,128]{1,0:T(8,128)}, u32[]{:S(2)}) copy-start(f32[1024,128]{1,0:T(8,128)} %copy-done.3) | copy-start | bytes 1572868
  140.5 13.3 %copy-start.12 = (f32[1,16,2,1]{2,1,3,0:T(8,128)S(1)}, f32[1,16,2,1]{2,1,3,0:T(8,128)}, u32[]{:S(2)}) copy-start(f32[1,16,2,1]{2,1,3,0:T(8,128)} %copy.89) | copy-start | bytes 388
  140.5 13.3 %copy-start.13 = (f32[2,16]{0,1:T(8,128)S(1)}, f32[2,16]{0,1:T(8,128)}, u32[]{:S(2)}) copy-start(f32[2,16]{0,1:T(8,128)} %copy.75) | copy-start | bytes 388
  140.5 13.3 %copy-start.14 = (f32[16,2]{1,0:T(8,128)S(1)}, f32[16,2]{1,0:T(8,128)}, u32[]{:S(2)}) copy-start(f32[16,2]{1,0:T(8,128)} %copy.73) | copy-start | bytes 388
  140.6 13.3 %copy-start.28 = (pred[2,2]{1,0:T(4,128)(4,1)S(1)}, pred[2,2]{1,0:T(4,128)(4,1)}, u32[]{:S(2)}) copy-start(pred[2,2]{1,0:T(4,128)(4,1)} %iota_compare_fusion.6) | copy-start | bytes 16
  140.6 12.1 %collective-permute-start.3 = (bf16[1040,128]{1,0:T(8,128)(2,1)}, bf16[1040,128]{1,0:T(8,128)(2,1)}, u32[]{:S(2)}, u32[]{:S(2)}) collective-permute-start(bf16[1040,128]{1,0:T(8,128)(2,1)} %fusion.65), channel_id=1, source_target_pairs={{0,16},{4,20},{8,24},{12,28},{1,17},{5,21},{9,25},{13,29},{2,18},{... | collective-permute-start | bytes 798728 | tf_op jit(solution)/shard_map/ppermute | solution.py:19
  160.5 3.3 %copy-start.26 = (f32[1024]{0:T(1024)S(1)}, f32[1024]{0:T(1024)}, u32[]{:S(2)}) copy-start(f32[1024]{0:T(1024)} %param.32) | copy-start | bytes 12292
  162.6 1.0 copy-start.8
  163.8 3.2 %copy-start.1 = (bf16[512,2048]{1,0:T(8,128)(2,1)S(1)}, bf16[512,2048]{1,0:T(8,128)(2,1)}, u32[]{:S(2)}) copy-start(bf16[512,2048]{1,0:T(8,128)(2,1)} %convolution_convert_fusion.2) | copy-start | bytes 6291460
  168.7 33.7 %copy-start.23 = (bf16[128,2]{0,1:T(2,128)(2,1)S(1)}, bf16[128,2]{0,1:T(2,128)(2,1)}, u32[]{:S(2)}) copy-start(bf16[128,2]{0,1:T(2,128)(2,1)} %param.37) | copy-start | bytes 1540
  168.7 33.8 %copy-start.20 = (s32[128,2]{0,1:T(2,128)S(1)}, s32[128,2]{0,1:T(2,128)}, u32[]{:S(2)}) copy-start(s32[128,2]{0,1:T(2,128)} %param.36) | copy-start | bytes 3076
  168.7 48.8 %copy-start.22 = (s32[24]{0:T(128)S(1)}, s32[24]{0:T(128)}, u32[]{:S(2)}) copy-start(s32[24]{0:T(128)} %copy-done.21) | copy-start | bytes 292
  198.8 23.5 %all-to-all-start.1 = ((bf16[8,24,2048]{2,1,0:T(8,128)(2,1)}), bf16[8,24,2048]{2,1,0:T(8,128)(2,1)S(1)}, u32[]{:S(2)}, u32[]{:S(2)}) async-start(bf16[8,24,2048]{2,1,0:T(8,128)(2,1)} %bitcast.302), calls=%async_computation.3 | async-start | bytes 1572864 | tf_op jit(solution)/shard_map/all_to_all | solution.py:273
Sparse Core Ops, SparseCore 0:
  10.8 25.2 all-gather.3
  40.7 27.5 all-gather.7
  69.9 28.4 all-gather.5
  100.8 37.9 reduce-scatter.7
  141.2 37.8 reduce-scatter.5
  181.4 34.4 reduce-scatter.3
where the time goes:
time: 233 us; the launch traced here: 232 us
  blocking collectives  80.4 us (35%)
  matrix products  57.2 us (25%)
  waiting for transfers between devices  35.4 us (15%)
  starting transfers between devices  22.3 us (10%)
  between operations  14.7 us (6%)
  other arithmetic  12.3 us (5%)
  local copies, waits for them, and re-layouts  9.4 us (4%)
    all_to_all x2, blocking collectives, local(): lax.all_to_all(block, 'ep', split_axis=0, concat_axis=0, tiled=True)  50.3 us
    all_to_all x1, blocking collectives, local(): lax.all_to_all(expert_rows(block), 'ep', split_axis=0, concat_axis=0, til...  30 us
    ppermute x4, starting transfers between devices, from_behind(): return lax.ppermute(value, axis, pairs)  18.3 us
    dot_general x2, matrix products, expert_rows(): jnp.einsum('osecf,efd->osecd', hidden, routed_down_weight, preferred_elem...  14.2 us
    reduce_scatter x1, waiting for transfers between devices, local(): lax.psum_scatter(jnp.concatenate([mix_term, moe_term], axis=1).reshape(tp...  13.4 us
    all_gather x2, waiting for transfers between devices, local(): gathered = [lax.all_gather(block, 'tp', axis=0) for block in arrived]  11.9 us
    dot_general x2, matrix products, expert_rows(): jnp.einsum('osecd,edf->osecf', sources, routed_gate_weight, preferred_ele...  8.17 us
    ppermute x4, waiting for transfers between devices, from_behind(): return lax.ppermute(value, axis, pairs)  6.87 us
  transfers between devices with their start and end apart: 11, of which 6 were waited for; matrix products, arithmetic and copies ran while one was open for 31% of the time, Pallas kernels for 0%

commit v1 on v0

--- a/solution.py
+++ b/solution.py
@@ -1,8 +1,13 @@
+import functools
+
 import jax
 import jax.numpy as jnp
 from jax import lax
+from jax.experimental import pallas as pl
+from jax.experimental.pallas import tpu as pltpu
 from jax.sharding import PartitionSpec as P
 
+MESH = pl.DeviceIdType.MESH
 HEAD_DIM = 64
 STATE = 128
 BLOCK = 64
@@ -294,6 +299,513 @@
     return (mixer_result.astype(jnp.bfloat16), moe_total.astype(jnp.bfloat16))
 
 
+def message_names(half):
+    names = ["meta_core", "meta_y", "meta_far", "rows_core", "rows_y", "rows_fwd", "shared", "dense", "mix_core", "mix_far", "mix_y"]
+    for d in range(half):
+        names += [f"{kind}{d}" for kind in ("a", "ay", "ac", "ra", "ry", "fa", "b", "bc", "rb", "fb")]
+    return {name: i for i, name in enumerate(names)}
+
+
+def exchange_kernel(
+    ep_count,
+    capacity,
+    rows_hbm,
+    meta_ref,
+    gain_ref,
+    mix_hbm,
+    gate_hbm,
+    up_hbm,
+    down_hbm,
+    sgate_hbm,
+    sup_hbm,
+    sdown_hbm,
+    mix_out,
+    moe_out,
+    rows_v,
+    mix_v,
+    gate_v,
+    up_v,
+    down_v,
+    sgate_v,
+    sup_v,
+    sdown_v,
+    meta_v,
+    grp,
+    pack_a,
+    pack_b,
+    xa,
+    xb,
+    ya,
+    yb,
+    ra,
+    rb,
+    sa,
+    sb,
+    ry,
+    fa,
+    ret_a,
+    ret_b,
+    sp,
+    rsp,
+    dense,
+    dense_s,
+    dense_r,
+    mix_r,
+    mix_s,
+    mix_ry,
+    load_sem,
+    send_sem,
+    recv_sem,
+):
+    half = ep_count // 2
+    cap = capacity
+    tok, width = rows_v.shape
+    col = 512
+    ids = message_names(half)
+    e = lax.axis_index("ep")
+    t = lax.axis_index("tp")
+    base = (e // half) * half
+    q = e - base
+    other = half - base
+    t_core = t + 1 - 2 * (t % 2)
+    t_y = (t + 2) % 4
+    t_far = (t_core + 2) % 4
+    core, ydev, far = (e, t_core), (e, t_y), (e, t_far)
+
+    def to_a(d):
+        return (other + (q + d) % half, t)
+
+    def from_a(d):
+        return (other + (q + half - d) % half, t)
+
+    def to_b(d):
+        return (base + (q + d) % half, t)
+
+    def from_b(d):
+        return (base + (q + half - d) % half, t)
+
+    loads = {}
+    for i, (name, src, dst) in enumerate(
+        (
+            ("rows", rows_hbm, rows_v),
+            ("sgate", sgate_hbm, sgate_v),
+            ("sup", sup_hbm, sup_v),
+            ("sdown", sdown_hbm, sdown_v),
+            ("gate", gate_hbm, gate_v),
+            ("up", up_hbm, up_v),
+            ("down", down_hbm, down_v),
+            ("mix", mix_hbm, mix_v),
+        )
+    ):
+        loads[name] = pltpu.make_async_copy(src, dst, load_sem.at[i])
+        loads[name].start()
+
+    copies = {}
+
+    def send(name, src, dst, device):
+        i = ids[name]
+        copies[name] = pltpu.make_async_remote_copy(
+            src_ref=src,
+            dst_ref=dst,
+            send_sem=send_sem.at[i],
+            recv_sem=recv_sem.at[i],
+            device_id=device,
+            device_id_type=MESH,
+        )
+        copies[name].start()
+
+    def arrived(name):
+        copies[name].wait_recv()
+
+    barrier = pltpu.get_barrier_semaphore()
+    peers = [core, ydev, far] + [to_a(d) for d in range(half)] + [to_b(d) for d in range(1, half)]
+    for peer in peers:
+        pl.semaphore_signal(barrier, inc=1, device_id=peer, device_id_type=MESH)
+
+    meta_v[0] = meta_ref[...]
+    loads["rows"].wait()
+
+    def norm_rows(i, carry):
+        at = pl.ds(pl.multiple_of(i * 16, 16), 16)
+        x = rows_v[at, :].astype(jnp.float32)
+        scale = lax.rsqrt(jnp.mean(x * x, axis=-1, keepdims=True) + eps_norm)
+        grp[0, at, :] = (x * scale * gain_ref[...]).astype(jnp.bfloat16)
+        return carry
+
+    lax.fori_loop(0, tok // 16, norm_rows, 0)
+    pl.semaphore_wait(barrier, len(peers))
+
+    send("meta_y", meta_v.at[0], meta_v.at[1], ydev)
+    send("meta_core", meta_v.at[0], meta_v.at[2], core)
+    send("meta_far", meta_v.at[0], meta_v.at[3], far)
+    send("rows_y", grp.at[0], grp.at[1], ydev)
+    send("rows_core", grp.at[0], grp.at[2], core)
+
+    def pack(pos, expert, put):
+        places = lax.broadcasted_iota(jnp.int32, (cap, tok), 0) + expert * cap
+        places = places.astype(jnp.float32)
+        chosen = (places == meta_v[pos, 0:1, :]) | (places == meta_v[pos, 1:2, :])
+        chosen = jnp.where(chosen, 1.0, 0.0).astype(jnp.bfloat16)
+        for n in range(0, width, col):
+            put(
+                n,
+                jnp.dot(chosen, grp[pos, :, n : n + col], preferred_element_type=jnp.float32).astype(
+                    jnp.bfloat16
+                ),
+            )
+
+    def put_in(ref, *lead):
+        def put(n, value):
+            ref[(*lead, slice(n, n + col))] = value
+
+        return put
+
+    for d in range(half):
+        pack(0, other + (q + d) % half, put_in(pack_a, d, slice(None)))
+        send(f"a{d}", pack_a.at[d], xa.at[d, pl.ds(0, cap)], to_a(d))
+
+    def shared_rows(pos):
+        x = grp[pos]
+        g = jnp.dot(x, sgate_v[...], preferred_element_type=jnp.float32)
+        u = jnp.dot(x, sup_v[...], preferred_element_type=jnp.float32)
+        h = (jax.nn.silu(g) * u).astype(jnp.bfloat16)
+        for n in range(0, width, col):
+            sp[pos, :, n : n + col] = jnp.dot(
+                h, sdown_v[:, n : n + col], preferred_element_type=jnp.float32
+            ).astype(jnp.bfloat16)
+
+    def expert(x_ref, y_ref):
+        x = x_ref[...]
+        g = jnp.dot(x, gate_v[...], preferred_element_type=jnp.float32)
+        u = jnp.dot(x, up_v[...], preferred_element_type=jnp.float32)
+        h = (jax.nn.silu(g) * u).astype(jnp.bfloat16)
+        for n in range(0, width, col):
+            y_ref[:, n : n + col] = jnp.dot(
+                h, down_v[:, n : n + col], preferred_element_type=jnp.float32
+            ).astype(jnp.bfloat16)
+
+    f32 = jnp.float32
+
+    def a1(d):
+        arrived(f"a{d}")
+        send(f"ay{d}", xa.at[d, pl.ds(0, cap)], xa.at[d, pl.ds(cap, cap)], ydev)
+
+    def a2(d):
+        arrived(f"ay{d}")
+        send(f"ac{d}", xa.at[d, pl.ds(0, 2 * cap)], xa.at[d, pl.ds(2 * cap, 2 * cap)], core)
+
+    def a3(d):
+        arrived(f"ac{d}")
+        expert(xa.at[d], ya.at[d])
+        send(f"ra{d}", ya.at[d, pl.ds(2 * cap, 2 * cap)], ra.at[d], core)
+
+    def a4(d):
+        arrived(f"ra{d}")
+        sa[d] = (ya[d, 0 : 2 * cap].astype(f32) + ra[d].astype(f32)).astype(jnp.bfloat16)
+        send(f"ry{d}", sa.at[d, pl.ds(cap, cap)], ry.at[d], ydev)
+
+    def a5(d):
+        arrived(f"ry{d}")
+        fa[d] = (sa[d, 0:cap].astype(f32) + ry[d].astype(f32)).astype(jnp.bfloat16)
+        send(f"fa{d}", fa.at[d], ret_a.at[pl.ds(d * cap, cap)], from_a(d))
+
+    def b1(d):
+        for p in range(2):
+            pack(p, base + (q + d) % half, put_in(pack_b, d - 1, slice(p * cap, (p + 1) * cap)))
+        send(f"b{d}", pack_b.at[d - 1], xb.at[d, pl.ds(0, 2 * cap)], to_b(d))
+
+    def b2(d):
+        arrived(f"b{d}")
+        send(f"bc{d}", xb.at[d, pl.ds(0, 2 * cap)], xb.at[d, pl.ds(2 * cap, 2 * cap)], core)
+
+    def b3(d):
+        if d:
+            arrived(f"bc{d}")
+        expert(xb.at[d], yb.at[d])
+        send(f"rb{d}", yb.at[d, pl.ds(2 * cap, 2 * cap)], rb.at[d], core)
+
+    def b4(d):
+        arrived(f"rb{d}")
+        for p in range(2):
+            at = slice(p * cap, (p + 1) * cap)
+            total = (yb[d, at].astype(f32) + rb[d, at].astype(f32)).astype(jnp.bfloat16)
+            if d:
+                sb[d - 1, p] = total
+            else:
+                ret_b[p, 0:cap] = total
+        if d:
+            send(f"fb{d}", sb.at[d - 1], ret_b.at[:, pl.ds(d * cap, cap)], from_b(d))
+
+    def chosen_slots(columns, first):
+        lanes = lax.broadcasted_iota(jnp.int32, (1, half * cap), 1)
+        code = lanes + (first + q) * cap
+        for d in range(1, half):
+            moved = (first + (q + d) % half - d) * cap
+            code = jnp.where(lanes >= d * cap, lanes + moved, code)
+        code = code.astype(f32)
+        return [jnp.where(columns[:, k : k + 1] == code, 1.0, 0.0).astype(jnp.bfloat16) for k in range(2)]
+
+    def mixed(columns, picks, returned):
+        total = None
+        for k in range(2):
+            part = columns[:, 2 + k : 3 + k] * jnp.dot(picks[k], returned, preferred_element_type=f32)
+            total = part if total is None else total + part
+        return total
+
+    def dense_rows(p):
+        columns = jnp.transpose(meta_v[p])
+        picks = chosen_slots(columns, base)
+        for n in range(0, width, col):
+            at = slice(n, n + col)
+            value = (
+                mixed(columns, picks, ret_b[p, :, at])
+                + sp[p, :, at].astype(f32)
+                + rsp[p, :, at].astype(f32)
+            )
+            if p:
+                dense_s[:, at] = value.astype(jnp.bfloat16)
+            else:
+                dense[:, at] = value
+
+    loads["sgate"].wait()
+    loads["sup"].wait()
+    loads["sdown"].wait()
+    shared_rows(0)
+    loads["mix"].wait()
+    send("mix_core", mix_v.at[t_core], mix_r.at[0], core)
+    send("mix_far", mix_v.at[t_far], mix_r.at[1], core)
+    arrived("meta_y")
+    arrived("rows_y")
+    send("rows_fwd", grp.at[1], grp.at[3], core)
+    for d in range(1, half):
+        b1(d)
+    arrived("meta_core")
+    arrived("meta_far")
+    arrived("rows_core")
+    shared_rows(1)
+    shared_rows(2)
+    for p in (0, 1, 2):
+        pack(p, e, put_in(xb, 0, slice(p * cap, (p + 1) * cap)))
+    a1(0)
+    arrived("rows_fwd")
+    shared_rows(3)
+    send("shared", sp.at[pl.ds(2, 2)], rsp, core)
+    pack(3, e, put_in(xb, 0, slice(3 * cap, 4 * cap)))
+    loads["gate"].wait()
+    loads["up"].wait()
+    loads["down"].wait()
+    b3(0)
+    a2(0)
+    b2(1)
+    a3(0)
+    a1(1)
+    b4(0)
+    a4(0)
+    b3(1)
+    a2(1)
+    b4(1)
+    b2(2)
+    a3(1)
+    a5(0)
+    a1(2)
+    a4(1)
+    b3(2)
+    a2(2)
+    b4(2)
+    b2(3)
+    a3(2)
+    a5(1)
+    a1(3)
+    a4(2)
+    b3(3)
+    a2(3)
+    b4(3)
+    a3(3)
+    a5(2)
+    a4(3)
+    a5(3)
+    arrived("mix_core")
+    arrived("mix_far")
+    mix_s[...] = (mix_v[t_y].astype(f32) + mix_r[1].astype(f32)).astype(jnp.bfloat16)
+    send("mix_y", mix_s, mix_ry, ydev)
+    for d in range(1, half):
+        arrived(f"fb{d}")
+    arrived("shared")
+    dense_rows(1)
+    send("dense", dense_s, dense_r, ydev)
+    dense_rows(0)
+    arrived("mix_y")
+    mix_out[...] = (
+        mix_v[t].astype(f32) + mix_r[0].astype(f32) + mix_ry[...].astype(f32)
+    ).astype(jnp.bfloat16)
+    for d in range(half):
+        arrived(f"fa{d}")
+    arrived("dense")
+    columns = jnp.transpose(meta_v[0])
+    picks = chosen_slots(columns, other)
+    for n in range(0, width, col):
+        at = slice(n, n + col)
+        value = mixed(columns, picks, ret_a[:, at]) + dense[:, at] + dense_r[:, at].astype(f32)
+        moe_out[:, at] = value.astype(jnp.bfloat16)
+    for name in copies:
+        copies[name].wait_send()
+
+
+def exchange(ep_count, capacity, rows, meta, gain, mix_term, gate, up, down, sgate, sup, sdown):
+    half = ep_count // 2
+    tok, width = rows.shape
+    bf16, f32 = jnp.bfloat16, jnp.float32
+    cap = capacity
+    mix_block = mix_term.shape[1]
+    count = len(message_names(half))
+    shapes = [
+        ((tok, width), bf16),
+        (mix_term.shape, bf16),
+        (gate.shape, bf16),
+        (up.shape, bf16),
+        (down.shape, bf16),
+        (sgate.shape, bf16),
+        (sup.shape, bf16),
+        (sdown.shape, bf16),
+        ((4, 8, tok), f32),
+        ((4, tok, width), bf16),
+        ((half, cap, width), bf16),
+        ((half - 1, 2 * cap, width), bf16),
+        ((half, 4 * cap, width), bf16),
+        ((half, 4 * cap, width), bf16),
+        ((half, 4 * cap, width), bf16),
+        ((half, 4 * cap, width), bf16),
+        ((half, 2 * cap, width), bf16),
+        ((half, 2 * cap, width), bf16),
+        ((half, 2 * cap, width), bf16),
+        ((half - 1, 2, cap, width), bf16),
+        ((half, cap, width), bf16),
+        ((half, cap, width), bf16),
+        ((half * cap, width), bf16),
+        ((2, half * cap, width), bf16),
+        ((4, tok, width), bf16),
+        ((2, tok, width), bf16),
+        ((tok, width), f32),
+        ((tok, width), bf16),
+        ((tok, width), bf16),
+        ((2, mix_block, width), bf16),
+        ((mix_block, width), bf16),
+        ((mix_block, width), bf16),
+    ]
+    any_spec = pl.BlockSpec(memory_space=pl.ANY)
+    vmem_spec = pl.BlockSpec(memory_space=pltpu.VMEM)
+    return pl.pallas_call(
+        functools.partial(exchange_kernel, ep_count, capacity),
+        out_shape=(
+            jax.ShapeDtypeStruct((mix_block, width), bf16),
+            jax.ShapeDtypeStruct((tok, width), bf16),
+        ),
+        in_specs=[any_spec, vmem_spec, vmem_spec] + [any_spec] * 7,
+        out_specs=(vmem_spec, vmem_spec),
+        scratch_shapes=[pltpu.VMEM(shape, dtype) for shape, dtype in shapes]
+        + [
+            pltpu.SemaphoreType.DMA((8,)),
+            pltpu.SemaphoreType.DMA((count,)),
+            pltpu.SemaphoreType.DMA((count,)),
+        ],
+        compiler_params=pltpu.CompilerParams(
+            collective_id=0, has_side_effects=True, vmem_limit_bytes=60 * 1024 * 1024
+        ),
+        name="moe_exchange",
+    )(rows, meta, gain, mix_term, gate, up, down, sgate, sup, sdown)
+
+
+def direct(
+    head_inputs_unfiltered,
+    group_write_vectors,
+    group_read_vectors,
+    output_gate_inputs,
+    step_preactivation,
+    extra_decay_logs,
+    head_decay_logs,
+    head_filter_taps,
+    write_filter_taps,
+    read_filter_taps,
+    grouped_norm_gain,
+    mixer_output_weight,
+    expert_input_rows,
+    expert_norm_gain,
+    routes,
+    router_chosen_scores,
+    routed_gate_weight,
+    routed_up_weight,
+    routed_down_weight,
+    shared_gate_weight,
+    shared_up_weight,
+    shared_down_weight,
+):
+    tp_count = lax.axis_size("tp")
+    ep_count = lax.axis_size("ep")
+    tok_local, model_width = expert_input_rows.shape
+    experts = ep_count
+    capacity = 3 * tok_local * routes.shape[1] // (2 * experts)
+    score_float = router_chosen_scores.astype(jnp.float32)
+    weights = score_float / jnp.sum(score_float, axis=1, keepdims=True) * route_scale
+    choice = routes[None, :, :] == jnp.arange(experts, dtype=jnp.int32)[:, None, None]
+    named = jnp.any(choice, axis=2)
+    row_order = jnp.arange(tok_local, dtype=jnp.int32)
+    earlier_rows = (row_order[:, None] < row_order[None, :]).astype(jnp.bfloat16)
+    rank = jnp.dot(named.astype(jnp.bfloat16), earlier_rows, preferred_element_type=jnp.float32)
+    place = jnp.sum(jnp.where(choice, rank[:, :, None], 0.0), axis=0) + (routes * capacity).astype(jnp.float32)
+    meta = jnp.pad(jnp.concatenate([place.T, weights.T], axis=0), ((0, 4), (0, 0)))
+
+    earlier = tail_rows_from_behind(
+        head_inputs_unfiltered, group_write_vectors, group_read_vectors, head_filter_taps.shape[0]
+    )
+    mixer_normed = mixer_rows(
+        earlier,
+        head_inputs_unfiltered,
+        group_write_vectors,
+        group_read_vectors,
+        output_gate_inputs,
+        step_preactivation,
+        extra_decay_logs,
+        head_decay_logs,
+        head_filter_taps,
+        write_filter_taps,
+        read_filter_taps,
+        grouped_norm_gain,
+    )
+    mix_block = mixer_normed.shape[0] // tp_count
+    mix_term = jnp.dot(
+        mixer_normed, mixer_output_weight, preferred_element_type=jnp.float32
+    ).astype(jnp.bfloat16).reshape(tp_count, mix_block, model_width)
+    return exchange(
+        ep_count,
+        capacity,
+        expert_input_rows,
+        meta,
+        expert_norm_gain.reshape(1, -1),
+        mix_term,
+        routed_gate_weight[0],
+        routed_up_weight[0],
+        routed_down_weight[0],
+        shared_gate_weight,
+        shared_up_weight,
+        shared_down_weight,
+    )
+
+
+def fits_direct(mesh, tok_local, top_count, local_experts):
+    ep_count = mesh.shape["ep"]
+    experts = ep_count * local_experts
+    capacity = 3 * tok_local * top_count // (2 * experts)
+    return (
+        mesh.shape["tp"] == 4
+        and ep_count % 2 == 0
+        and ep_count <= 8
+        and local_experts == 1
+        and top_count == 2
+        and capacity % 16 == 0
+        and tok_local == 128
+    )
+
+
 def solution(mesh):
     in_specs = (
         P("ep", "tp"),
@@ -320,4 +832,15 @@
         P("tp", None),
     )
     out_specs = (P(("ep", "tp"), None), P(("ep", "tp"), None))
-    return jax.shard_map(local, mesh=mesh, in_specs=in_specs, out_specs=out_specs, check_vma=False)
+    def step(*args):
+        devices = mesh.shape["ep"] * mesh.shape["tp"]
+        body = (
+            direct
+            if fits_direct(mesh, args[12].shape[0] // devices, args[14].shape[1], args[16].shape[0] // mesh.shape["ep"])
+            else local
+        )
+        return jax.shard_map(
+            body, mesh=mesh, in_specs=in_specs, out_specs=out_specs, check_vma=False
+        )(*args)
+
+    return step

time: 233 us -> 171 us (0.73)
  Pallas kernels: 0 us -> 100 us
  blocking collectives: 80.4 us -> 0 us
  matrix products: 57.2 us -> 17.7 us
  waiting for transfers between devices: 35.4 us -> 12.1 us
  between operations: 14.7 us -> 1 us
  starting transfers between devices: 22.3 us -> 19.3 us
    pallas_call x0 -> x1, Pallas kernels: none -> 100 us  [exchange(): pl.pallas_call(functools.partial(exchange_kernel, ep_count, capacity), ou...]
    all_to_all x3 -> x0, blocking collectives: 80.4 us -> none  [the longest x2 50.3 us: local(): lax.all_to_all(block, 'ep', split_axis=0, concat_axis=0, tiled=True)]
    dot_general x12 -> x2, matrix products: 40.6 us -> 3.97 us  [the longest x1 3.84 us: direct(): jnp.dot(mixer_normed, mixer_output_weight, preferred_element_type=jnp.flo...]
    reduce_scatter x3 -> x0, waiting for transfers between devices: 13.5 us -> none  [the longest x1 13.4 us: local(): lax.psum_scatter(jnp.concatenate([mix_term, moe_term], axis=1).reshape(tp...]
    all_gather x3 -> x0, waiting for transfers between devices: 11.9 us -> none  [the longest x2 11.9 us: local(): gathered = [lax.all_gather(block, 'tp', axis=0) for block in arrived]]
    ppermute x4, waiting for transfers between devices: 6.87 us -> 12.1 us  [from_behind(): return lax.ppermute(value, axis, pairs)]
    all_to_all x1 -> x0, starting transfers between devices: 3.64 us -> none  [local(): lax.all_to_all(expert_rows(block), 'ep', split_axis=0, concat_axis=0, til...]
    all_to_all x1 -> x0, waiting for transfers between devices: 3 us -> none  [local(): lax.all_to_all(expert_rows(block), 'ep', split_axis=0, concat_axis=0, til...]
  transfers between devices with their start and end apart: 11 -> 4, of which waited for: 6 -> 3; matrix products, arithmetic and copies ran while one was open for 31% -> 6% of each run, Pallas kernels for 0% -> 0%
where the time goes in v1:
time: 171 us; the launch traced here: 170 us
  Pallas kernels  100 us (58%)
  starting transfers between devices  19.3 us (11%)
  matrix products  17.7 us (10%)
  waiting for transfers between devices  12.1 us (7%)
  other arithmetic  11.2 us (7%)
  local copies, waits for them, and re-layouts  8.42 us (5%)
    pallas_call x1, Pallas kernels, exchange(): pl.pallas_call(functools.partial(exchange_kernel, ep_count, capacity), ou...  100 us
    ppermute x4, starting transfers between devices, from_behind(): return lax.ppermute(value, axis, pairs)  19.3 us
    ppermute x4, waiting for transfers between devices, from_behind(): return lax.ppermute(value, axis, pairs)  12.1 us
    dot_general x1, matrix products, mixer_rows(): jnp.einsum('gebc,cgepn->bgepn', carry_weights, block_states, precision=hi...  5.58 us
    dot_general x1, matrix products, direct(): jnp.dot(mixer_normed, mixer_output_weight, preferred_element_type=jnp.flo...  3.84 us
    dot_general x1, matrix products, mixer_rows(): jnp.einsum('gec,cgepn->gepn', jnp.exp(device_decay[..., None] - running),...  3.81 us
    unnamed x15, local copies, waits for them, and re-layouts  3.76 us
  transfers between devices with their start and end apart: 4, of which 3 were waited for; matrix products, arithmetic and copies ran while one was open for 6% of the time, Pallas kernels for 0%

profile of v1, /device:TPU:0, one launch (start us, length us, event | category | flops | bytes accessed | tf_op | source)
XLA Modules:
  0.0 169.8 jit_solution(18308539828519134706)
XLA Ops:
  0.6 0.0 copy-start.3
  0.6 0.0 copy-start.2
  0.7 0.7 slice.107
  1.4 0.7 slice.106
  2.1 0.7 slice.105
  2.8 4.9 %collective-permute-start = (bf16[3,1280]{1,0:T(4,128)(2,1)S(1)}, bf16[3,1280]{1,0:T(4,128)(2,1)S(1)}, u32[]{:S(2)}, u32[]{:S(2)}) collective-permute-start(bf16[3,1280]{1,0:T(4,128)(2,1)S(1)} %pad_maximum_fusion.3), channel_id=1, source_target_pairs={{0,4},{4,8},{8,12},{12,16},{16,20},{20,24},{24,28},{1,5},{5,9},{9,... | collective-permute-start | bytes 23048 | tf_op jit(solution)/shard_map/ppermute | solution.py:24
  7.7 0.7 exponential_negate_fusion
  8.4 0.8 compare_select_fusion
  9.1 0.1 reshape.371
  9.2 0.5 reduce_window_sum.24
  9.7 0.2 slice_reduce_fusion
  9.9 0.1 subtract_exponential_fusion
  10.0 0.7 convert_reduce_fusion
  10.7 0.7 fusion.51
  11.4 0.1 fusion.38
  11.5 0.7 select_reduce_fusion
  12.2 0.8 bitcast_convert_fusion.3
  13.0 0.8 bitcast_convert_fusion.7
  13.9 0.9 slice_convert_fusion.3
  14.7 0.7 fusion.53
  15.5 0.1 reshape.368
  15.6 0.1 copy.70
  15.7 0.1 copy.66
  15.7 0.0 collective-permute-done
  15.8 1.8 %divide_multiply_fusion = f32[128,1024]{1,0:T(8,128)S(1)} fusion(bf16[128,1024]{1,0:T(8,128)(2,1)} %param.22, bf16[3,1024]{1,0:T(4,128)(2,1)S(1)} %slice.138, f32[1024]{0:T(1024)S(1)} %bitcast.178, f32[1024]{0:T(1024)S(1)} %bitcast.179, f32[1024]{0:T(1024)S(1)} %bitcast.177, f32[1024]{0:T(1024)S(1)} %bitcast.176), kind=kLoop, calls=%fused_computation.44 | loop fusion | flops 3145728 | bytes 808960 | tf_op jit(solution)/shard_map/jit(silu)/mul | solution.py:69
  17.6 0.3 reshape.367
  17.9 0.4 copy.52
  18.3 0.0 copy-done.3
  18.4 0.1 divide_multiply_fusion.1
  18.5 1.1 fusion.4
  19.6 3.8 %fusion.12 = f32[16,1,64,128]{3,1,2,0:T(1,128)S(1)} fusion(f32[16,2,1,1]{1,2,3,0:T(1,128)S(1)} %copy.66, f32[2,16,64,128]{3,2,1,0:T(8,128)S(1)} %fusion.4), kind=kOutput, calls=%fused_computation.17 | convolution fusion | flops 3145728 | bytes 1572992 | tf_op jit(solution)/shard_map/gec,cgepn->gepn/dot_general | solution.py:141
  23.5 3.5 %collective-permute-start.1 = (bf16[1040,128]{1,0:T(8,128)(2,1)S(1)}, bf16[1040,128]{1,0:T(8,128)(2,1)S(1)}, u32[]{:S(2)}, u32[]{:S(2)}) collective-permute-start(bf16[1040,128]{1,0:T(8,128)(2,1)S(1)} %fusion.31), channel_id=1, source_target_pairs={{0,4},{4,8},{8,12},{12,16},{16,20},{20,24},{24,28},{1,5},{5,9},{9,... | collective-permute-start | bytes 798728 | tf_op jit(solution)/shard_map/ppermute | solution.py:24
  27.0 0.1 iota_compare_fusion.6
  27.0 5.3 %collective-permute-done.1 = bf16[1040,128]{1,0:T(8,128)(2,1)S(1)} collective-permute-done((bf16[1040,128]{1,0:T(8,128)(2,1)S(1)}, bf16[1040,128]{1,0:T(8,128)(2,1)S(1)}, u32[]{:S(2)}, u32[]{:S(2)}) %collective-permute-start.1) | collective-permute-done | bytes 266272 | tf_op jit(solution)/shard_map/ppermute | solution.py:24
  32.3 0.1 slice_reduce_fusion.2
  32.5 0.1 copy.71
  32.6 0.1 add_convert_fusion.1
  32.8 5.3 %collective-permute-start.2 = (bf16[1040,128]{1,0:T(8,128)(2,1)S(1)}, bf16[1040,128]{1,0:T(8,128)(2,1)S(1)}, u32[]{:S(2)}, u32[]{:S(2)}) collective-permute-start(bf16[1040,128]{1,0:T(8,128)(2,1)S(1)} %fusion.32), channel_id=1, source_target_pairs={{0,8},{4,12},{8,16},{12,20},{16,24},{20,28},{1,9},{5,13},{9,17},{1... | collective-permute-start | bytes 798728 | tf_op jit(solution)/shard_map/ppermute | solution.py:24
  38.1 0.1 copy.54
  38.2 0.1 slice_subtract_fusion
  38.3 4.3 %collective-permute-done.2 = bf16[1040,128]{1,0:T(8,128)(2,1)S(1)} collective-permute-done((bf16[1040,128]{1,0:T(8,128)(2,1)S(1)}, bf16[1040,128]{1,0:T(8,128)(2,1)S(1)}, u32[]{:S(2)}, u32[]{:S(2)}) %collective-permute-start.2) | collective-permute-done | bytes 266272 | tf_op jit(solution)/shard_map/ppermute | solution.py:24
  42.6 0.1 slice_reduce_fusion.1
  42.8 0.1 copy.72
  42.9 0.2 add_convert_fusion
  43.2 5.6 %collective-permute-start.3 = (bf16[1040,128]{1,0:T(8,128)(2,1)S(1)}, bf16[1040,128]{1,0:T(8,128)(2,1)S(1)}, u32[]{:S(2)}, u32[]{:S(2)}) collective-permute-start(bf16[1040,128]{1,0:T(8,128)(2,1)S(1)} %fusion.33), channel_id=1, source_target_pairs={{0,16},{4,20},{8,24},{12,28},{1,17},{5,21},{9,25},{13,29},{2,18},{... | collective-permute-start | bytes 798728 | tf_op jit(solution)/shard_map/ppermute | solution.py:24
  48.8 0.6 select_maximum_fusion.meta_ref
  49.4 0.1 copy.58
  49.4 0.1 copy.56
  49.5 0.2 copy.69
  49.7 0.2 fusion.66
  50.0 2.5 %collective-permute-done.3 = bf16[1040,128]{1,0:T(8,128)(2,1)S(1)} collective-permute-done((bf16[1040,128]{1,0:T(8,128)(2,1)S(1)}, bf16[1040,128]{1,0:T(8,128)(2,1)S(1)}, u32[]{:S(2)}, u32[]{:S(2)}) %collective-permute-start.3) | collective-permute-done | bytes 266272 | tf_op jit(solution)/shard_map/ppermute | solution.py:24
  52.5 0.2 fusion.22
  52.7 5.6 %fusion.3 = f32[2,16,64,128]{3,0,2,1:T(2,128)S(1)} fusion(f32[2,16,64,128]{3,2,1,0:T(8,128)} %copy-done, f32[16,64,128]{2,1,0:T(8,128)S(1)} %fusion.22, f32[2,16]{0,1:T(8,128)S(1)} %copy.58, pred[2,2]{1,0:T(4,128)(4,1)S(1)} %iota_compare_fusion.6, f32[16,2]{1,0:T(8,128)S(1)} %copy.56, f32[16,2]{1,0:T(8,128)S(1)} %bitcast.182), kind=kOutput, calls=%fused_computation.7 | convolution fusion | flops 6815872 | bytes 2621828 | tf_op jit(solution)/shard_map/gebc,cgepn->bgepn/dot_general | solution.py:139
  58.3 0.0 copy-start.1
  58.3 1.0 fusion.1
  59.3 0.0 copy-start.4
  59.3 2.0 %fusion = f32[2,64,1,16,64]{1,4,3,0,2:T(8,128)S(1)} fusion(f32[2,64,1,16,64]{1,4,3,0,2:T(8,128)S(1)} %fusion.1, f32[2,64,16,64]{1,3,2,0:T(8,128)S(1)} %copy.52, f32[16,2,64]{2,0,1:T(8,128)S(1)} %bitcast.167, f32[2,64,64]{2,1,0:T(8,128)S(1)} %fusion.66, f32[2,64,16]{1,2,0:T(8,128)S(1)} %copy.51, pred[64,64]{1,0:T(8,128)(4,1)S(1)} %iota_compare_fusion.3), kind=kOutput, calls=%fused_computation.4 | convolution fusion | flops 101318656 | bytes 1626112 | tf_op jit(solution)/shard_map/gebls,bsgep->blgep/dot_general | solution.py:126
  61.3 0.5 copy.63
  61.9 0.3 reshape.379
  62.2 0.2 multiply_reduce_fusion
  62.5 3.8 %convolution_convert_fusion = bf16[128,2048]{1,0:T(8,128)(2,1)} fusion(bf16[1024,2048]{1,0:T(8,128)(2,1)} %param.33, f32[1024]{0:T(1024)S(1)} %copy-done.4, f32[128]{0:T(128)S(1)} %add_rsqrt_fusion, f32[128,1024]{1,0:T(8,128)S(1)} %reshape.379, bf16[128,1024]{1,0:T(8,128)(2,1)S(1)} %copy-done.1), kind=kOutput, calls=%fused_computation | convolution fusion | flops 538312704 | bytes 5509632 | tf_op jit(solution)/shard_map/dot_general | solution.py:775
  66.3 100.0 %moe_exchange.1 = (bf16[32,2048]{1,0:T(8,128)(2,1)}, bf16[128,2048]{1,0:T(8,128)(2,1)}) custom-call(bf16[128,2048]{1,0:T(8,128)(2,1)} %rows_hbm.1, f32[8,128]{1,0:T(8,128)} %select_maximum_fusion.meta_ref, f32[1,2048]{1,0:T(1,128)} %bitcast.181, bf16[4,32,2048]{2,1,0:T(8,128)(2,1)} %bitcast.172, bf16[2048,256]{1,0:T(8,128)(2,1)} %bitcast.160, ...), custom_call_target="tpu_custom_call" | custom-call | tf_op jit(solution)/shard_map/moe_exchange/pallas_call | solution.py:697
  166.3 1.6 copy.81
  167.9 1.9 %copy.82 = bf16[128,2048]{1,0:T(8,128)(2,1)} copy(bf16[128,2048]{1,0:T(8,128)(2,1)} %get-tuple-element.37) | data formatting | bytes 1048576
  (36 shorter events, 0.5 us)
Async XLA Ops:
  0.6 17.7 %copy-start.3 = (bf16[128,128]{1,0:T(8,128)(2,1)S(1)}, bf16[128,128]{1,0:T(8,128)(2,1)}, u32[]{:S(2)}) copy-start(bf16[128,128]{1,0:T(8,128)(2,1)} %param.24) | copy-start | bytes 98308
  0.6 17.7 %copy-start.2 = (bf16[128,128]{1,0:T(8,128)(2,1)S(1)}, bf16[128,128]{1,0:T(8,128)(2,1)}, u32[]{:S(2)}) copy-start(bf16[128,128]{1,0:T(8,128)(2,1)} %param.23) | copy-start | bytes 98308
  2.8 12.9 %collective-permute-start = (bf16[3,1280]{1,0:T(4,128)(2,1)S(1)}, bf16[3,1280]{1,0:T(4,128)(2,1)S(1)}, u32[]{:S(2)}, u32[]{:S(2)}) collective-permute-start(bf16[3,1280]{1,0:T(4,128)(2,1)S(1)} %pad_maximum_fusion.3), channel_id=1, source_target_pairs={{0,4},{4,8},{8,12},{12,16},{16,20},{20,24},{24,28},{1,5},{5,9},{9,... | collective-permute-start | bytes 23048 | tf_op jit(solution)/shard_map/ppermute | solution.py:24
  19.6 12.7 %copy-start = (f32[2,16,64,128]{3,2,1,0:T(8,128)}, f32[2,16,64,128]{3,2,1,0:T(8,128)S(1)}, u32[]{:S(2)}) copy-start(f32[2,16,64,128]{3,2,1,0:T(8,128)S(1)} %fusion.4) | copy-start | bytes 3145732
  23.5 8.8 %collective-permute-start.1 = (bf16[1040,128]{1,0:T(8,128)(2,1)S(1)}, bf16[1040,128]{1,0:T(8,128)(2,1)S(1)}, u32[]{:S(2)}, u32[]{:S(2)}) collective-permute-start(bf16[1040,128]{1,0:T(8,128)(2,1)S(1)} %fusion.31), channel_id=1, source_target_pairs={{0,4},{4,8},{8,12},{12,16},{16,20},{20,24},{24,28},{1,5},{5,9},{9,... | collective-permute-start | bytes 798728 | tf_op jit(solution)/shard_map/ppermute | solution.py:24
  32.8 9.8 %collective-permute-start.2 = (bf16[1040,128]{1,0:T(8,128)(2,1)S(1)}, bf16[1040,128]{1,0:T(8,128)(2,1)S(1)}, u32[]{:S(2)}, u32[]{:S(2)}) collective-permute-start(bf16[1040,128]{1,0:T(8,128)(2,1)S(1)} %fusion.32), channel_id=1, source_target_pairs={{0,8},{4,12},{8,16},{12,20},{16,24},{20,28},{1,9},{5,13},{9,17},{1... | collective-permute-start | bytes 798728 | tf_op jit(solution)/shard_map/ppermute | solution.py:24
  43.2 9.3 %collective-permute-start.3 = (bf16[1040,128]{1,0:T(8,128)(2,1)S(1)}, bf16[1040,128]{1,0:T(8,128)(2,1)S(1)}, u32[]{:S(2)}, u32[]{:S(2)}) collective-permute-start(bf16[1040,128]{1,0:T(8,128)(2,1)S(1)} %fusion.33), channel_id=1, source_target_pairs={{0,16},{4,20},{8,24},{12,28},{1,17},{5,21},{9,25},{13,29},{2,18},{... | collective-permute-start | bytes 798728 | tf_op jit(solution)/shard_map/ppermute | solution.py:24
  58.3 3.9 %copy-start.1 = (bf16[128,1024]{1,0:T(8,128)(2,1)S(1)}, bf16[128,1024]{1,0:T(8,128)(2,1)}, u32[]{:S(2)}) copy-start(bf16[128,1024]{1,0:T(8,128)(2,1)} %param.25) | copy-start | bytes 786436
  59.3 3.2 %copy-start.4 = (f32[1024]{0:T(1024)S(1)}, f32[1024]{0:T(1024)}, u32[]{:S(2)}) copy-start(f32[1024]{0:T(1024)} %param.32) | copy-start | bytes 12292

commit v2 on v1

--- a/solution.py
+++ b/solution.py
@@ -301,6 +301,9 @@
 
 def message_names(half):
     names = ["meta_core", "meta_y", "meta_far", "rows_core", "rows_y", "rows_fwd", "shared", "dense", "mix_core", "mix_far", "mix_y"]
+    names += ["halo_h", "halo_w", "halo_r"]
+    for r in range((2 * half - 1).bit_length()):
+        names += [f"state{r}", f"decay{r}"]
     for d in range(half):
         names += [f"{kind}{d}" for kind in ("a", "ay", "ac", "ra", "ry", "fa", "b", "bc", "rb", "fb")]
     return {name: i for i, name in enumerate(names)}
@@ -312,7 +315,18 @@
     rows_hbm,
     meta_ref,
     gain_ref,
-    mix_hbm,
+    heads_hbm,
+    write_hbm,
+    read_hbm,
+    ogate_hbm,
+    proj_hbm,
+    step_ref,
+    extra_ref,
+    decay_ref,
+    htaps_ref,
+    wtaps_ref,
+    rtaps_ref,
+    mgain_ref,
     gate_hbm,
     up_hbm,
     down_hbm,
@@ -323,6 +337,29 @@
     moe_out,
     rows_v,
     mix_v,
+    heads_v,
+    write_v,
+    read_v,
+    ogate_v,
+    proj_v,
+    halo_h,
+    halo_w,
+    halo_r,
+    ext_h,
+    ext_w,
+    ext_r,
+    hval,
+    y_v,
+    read_b,
+    grow_v,
+    own_s,
+    own_d,
+    bef_s,
+    bef_d,
+    out_s,
+    out_d,
+    in_s,
+    in_d,
     gate_v,
     up_v,
     down_v,
@@ -360,6 +397,9 @@
     half = ep_count // 2
     cap = capacity
     tok, width = rows_v.shape
+    tok_m, chans = heads_v.shape
+    heads = step_ref.shape[0]
+    head_dim = chans // heads
     col = 512
     ids = message_names(half)
     e = lax.axis_index("ep")
@@ -394,7 +434,11 @@
             ("gate", gate_hbm, gate_v),
             ("up", up_hbm, up_v),
             ("down", down_hbm, down_v),
-            ("mix", mix_hbm, mix_v),
+            ("heads", heads_hbm, heads_v),
+            ("write", write_hbm, write_v),
+            ("read", read_hbm, read_v),
+            ("ogate", ogate_hbm, ogate_v),
+            ("proj", proj_hbm, proj_v),
         )
     ):
         loads[name] = pltpu.make_async_copy(src, dst, load_sem.at[i])
@@ -402,7 +446,7 @@
 
     copies = {}
 
-    def send(name, src, dst, device):
+    def prepare(name, src, dst, device):
         i = ids[name]
         copies[name] = pltpu.make_async_remote_copy(
             src_ref=src,
@@ -412,6 +456,9 @@
             device_id=device,
             device_id_type=MESH,
         )
+
+    def send(name, src, dst, device):
+        prepare(name, src, dst, device)
         copies[name].start()
 
     def arrived(name):
@@ -423,6 +470,7 @@
         pl.semaphore_signal(barrier, inc=1, device_id=peer, device_id_type=MESH)
 
     meta_v[0] = meta_ref[...]
+    f32, bf16 = jnp.float32, jnp.bfloat16
     loads["rows"].wait()
 
     def norm_rows(i, carry):
@@ -440,6 +488,16 @@
     send("meta_far", meta_v.at[0], meta_v.at[3], far)
     send("rows_y", grp.at[0], grp.at[1], ydev)
     send("rows_core", grp.at[0], grp.at[2], core)
+
+
+    nxt = ((e + 1) % ep_count, t)
+    halo_rows = halo_h.shape[0]
+    tail = pl.ds(tok_m - halo_rows, halo_rows)
+    for name in ("heads", "write", "read"):
+        loads[name].wait()
+    send("halo_h", heads_v.at[tail], halo_h, nxt)
+    send("halo_w", write_v.at[tail], halo_w, nxt)
+    send("halo_r", read_v.at[tail], halo_r, nxt)
 
     def pack(pos, expert, put):
         places = lax.broadcasted_iota(jnp.int32, (cap, tok), 0) + expert * cap
@@ -483,8 +541,6 @@
             y_ref[:, n : n + col] = jnp.dot(
                 h, down_v[:, n : n + col], preferred_element_type=jnp.float32
             ).astype(jnp.bfloat16)
-
-    f32 = jnp.float32
 
     def a1(d):
         arrived(f"a{d}")
@@ -567,13 +623,143 @@
             else:
                 dense[:, at] = value
 
+
+    def conv(x_v, halo, ext, taps_ref, n, size):
+        at = slice(n, n + size)
+        taps = taps_ref.shape[0]
+        edge = ext.shape[0] - tok_m
+        first = halo.shape[0] - edge
+        there = jnp.where(e > 0, 1.0, 0.0).astype(f32)
+        ext[0:edge, at] = halo[first:, at].astype(f32) * there
+        ext[edge:, at] = x_v[:, at].astype(f32)
+        total = None
+        for j in range(taps):
+            low = edge - taps + 1 + j
+            part = taps_ref[j : j + 1, at].astype(f32) * ext[low : low + tok_m, at]
+            total = part if total is None else total + part
+        return jax.nn.silu(total)
+
+    head_row = lax.broadcasted_iota(jnp.int32, (heads, chans), 0)
+    lane_head = lax.broadcasted_iota(jnp.int32, (heads, chans), 1) - head_row * head_dim
+    spread_b = jnp.where((lane_head >= 0) & (lane_head < head_dim), 1.0, 0.0).astype(bf16)
+
+    def spread(value, terms):
+        total, rest = None, value
+        for _ in range(terms):
+            part = rest.astype(bf16)
+            rest = rest - part.astype(f32)
+            add = jnp.dot(part, spread_b, preferred_element_type=f32)
+            total = add if total is None else total + add
+        return total
+
+    def mixer_local():
+        for name in ("halo_h", "halo_w", "halo_r"):
+            arrived(name)
+        for n in range(0, chans, 256):
+            hval[:, n : n + 256] = conv(heads_v, halo_h, ext_h, htaps_ref, n, 256)
+        states = write_v.shape[1]
+        write = conv(write_v, halo_w, ext_w, wtaps_ref, 0, states)
+        read = conv(read_v, halo_r, ext_r, rtaps_ref, 0, states)
+        read_b[...] = read.astype(bf16)
+        step = jax.nn.softplus(step_ref[...])
+        rate = step * -jnp.exp(decay_ref[...]) + extra_ref[...]
+        row = lax.broadcasted_iota(jnp.int32, (tok_m, tok_m), 0)
+        lane = lax.broadcasted_iota(jnp.int32, (tok_m, tok_m), 1)
+        upto = jnp.where(row <= lane, 1.0, 0.0).astype(f32)
+        cum = jnp.dot(rate, upto, precision=highest, preferred_element_type=f32)
+        cum_t = jnp.transpose(cum)
+        to_end = jnp.exp(cum[:, tok_m - 1 : tok_m] - cum) * step
+        affinity = lax.dot_general(
+            read, write, (((1,), (1,)), ((), ())), precision=highest, preferred_element_type=f32
+        )
+        weights = spread(jnp.transpose(to_end), 2)
+        weighted = (hval[...] * weights).astype(bf16)
+        own_s[...] = jnp.dot(
+            jnp.transpose(write).astype(bf16), weighted, preferred_element_type=f32
+        )
+        own_d[...] = jnp.broadcast_to(spread(cum_t[tok_m - 8 : tok_m], 3)[7:8], own_d.shape)
+        state_send(0)
+        grow_v[...] = spread(jnp.exp(cum_t), 2)
+        causal = row >= lane
+        for pair in range(heads // 2):
+            at = slice(pair * 2 * head_dim, (pair + 1) * 2 * head_dim)
+            parts = []
+            for h in (2 * pair, 2 * pair + 1):
+                gap = jnp.where(causal, cum_t[:, h : h + 1] - cum[h : h + 1, :], -jnp.inf)
+                parts.append((affinity * jnp.exp(gap) * step[h : h + 1, :]).astype(bf16))
+            both = hval[:, at].astype(bf16)
+            side = lax.broadcasted_iota(jnp.int32, both.shape, 1) < head_dim
+            zero = jnp.zeros_like(both)
+            y_v[:, at] = jnp.dot(
+                parts[0], jnp.where(side, both, zero), preferred_element_type=f32
+            ) + jnp.dot(parts[1], jnp.where(side, zero, both), preferred_element_type=f32)
+
+    rounds = (ep_count - 1).bit_length()
+
+    def state_send(r):
+        by = 2**r
+        if r == 0:
+            out_s[r] = own_s[...].astype(bf16)
+            out_d[r] = own_d[...]
+        else:
+            grown = jnp.exp(own_d[0:1, :])
+            out_s[r] = (own_s[...] + grown * bef_s[...]).astype(bf16)
+            out_d[r] = own_d[...] + bef_d[...]
+
+        later = ((e + by) % ep_count, t)
+        prepare(f"state{r}", out_s.at[r], in_s.at[r], later)
+        prepare(f"decay{r}", out_d.at[r], in_d.at[r], later)
+
+        @pl.when(e + by < ep_count)
+        def _():
+            copies[f"state{r}"].start()
+            copies[f"decay{r}"].start()
+
+    def state_arrive(r):
+        by = 2**r
+
+        @pl.when(e < by)
+        def _():
+            in_s[r] = jnp.zeros(in_s.shape[1:], bf16)
+            in_d[r] = jnp.zeros(in_d.shape[1:], f32)
+
+        @pl.when(e >= by)
+        def _():
+            arrived(f"state{r}")
+            arrived(f"decay{r}")
+
+        if r == 0:
+            bef_s[...] = in_s[0].astype(f32)
+            bef_d[...] = in_d[0]
+        else:
+            bef_s[...] = bef_s[...] + jnp.exp(bef_d[0:1, :]) * in_s[r].astype(f32)
+            bef_d[...] = bef_d[...] + in_d[r]
+        if r + 1 < rounds:
+            state_send(r + 1)
+
+    def mixer_finish():
+        square = jnp.zeros((tok_m, 1), f32)
+        for n in range(0, chans, 256):
+            at = slice(n, n + 256)
+            carried = jnp.dot(read_b[...], bef_s[:, at].astype(bf16), preferred_element_type=f32)
+            value = (y_v[:, at] + carried * grow_v[:, at]) * jax.nn.silu(ogate_v[:, at].astype(f32))
+            y_v[:, at] = value
+            square = square + jnp.sum(value * value, axis=-1, keepdims=True)
+        scale = lax.rsqrt(square / chans + eps_norm)
+        normed = (y_v[...] * scale * mgain_ref[...]).astype(bf16)
+        block = mix_v.shape[1]
+        for n in range(0, width, col):
+            part = jnp.dot(normed, proj_v[:, n : n + col], preferred_element_type=f32).astype(bf16)
+            for i in range(4):
+                mix_v[i, :, n : n + col] = part[i * block : (i + 1) * block]
+        send("mix_core", mix_v.at[t_core], mix_r.at[0], core)
+        send("mix_far", mix_v.at[t_far], mix_r.at[1], core)
+
     loads["sgate"].wait()
     loads["sup"].wait()
     loads["sdown"].wait()
     shared_rows(0)
-    loads["mix"].wait()
-    send("mix_core", mix_v.at[t_core], mix_r.at[0], core)
-    send("mix_far", mix_v.at[t_far], mix_r.at[1], core)
+    mixer_local()
     arrived("meta_y")
     arrived("rows_y")
     send("rows_fwd", grp.at[1], grp.at[3], core)
@@ -582,23 +768,24 @@
     arrived("meta_core")
     arrived("meta_far")
     arrived("rows_core")
+    a1(0)
     shared_rows(1)
     shared_rows(2)
     for p in (0, 1, 2):
         pack(p, e, put_in(xb, 0, slice(p * cap, (p + 1) * cap)))
-    a1(0)
     arrived("rows_fwd")
     shared_rows(3)
     send("shared", sp.at[pl.ds(2, 2)], rsp, core)
     pack(3, e, put_in(xb, 0, slice(3 * cap, 4 * cap)))
+    a2(0)
     loads["gate"].wait()
     loads["up"].wait()
     loads["down"].wait()
     b3(0)
-    a2(0)
-    b2(1)
+    state_arrive(0)
     a3(0)
     a1(1)
+    b2(1)
     b4(0)
     a4(0)
     b3(1)
@@ -607,6 +794,7 @@
     b2(2)
     a3(1)
     a5(0)
+    state_arrive(1)
     a1(2)
     a4(1)
     b3(2)
@@ -620,8 +808,12 @@
     b3(3)
     a2(3)
     b4(3)
+    state_arrive(2)
     a3(3)
     a5(2)
+    loads["ogate"].wait()
+    loads["proj"].wait()
+    mixer_finish()
     a4(3)
     a5(3)
     arrived("mix_core")
@@ -647,20 +839,55 @@
         at = slice(n, n + col)
         value = mixed(columns, picks, ret_a[:, at]) + dense[:, at] + dense_r[:, at].astype(f32)
         moe_out[:, at] = value.astype(jnp.bfloat16)
+    for r in range(rounds):
+
+        @pl.when(e + 2**r < ep_count)
+        def _():
+            copies[f"state{r}"].wait_send()
+            copies[f"decay{r}"].wait_send()
+
     for name in copies:
-        copies[name].wait_send()
-
-
-def exchange(ep_count, capacity, rows, meta, gain, mix_term, gate, up, down, sgate, sup, sdown):
+        if not name.startswith(("state", "decay")):
+            copies[name].wait_send()
+
+
+def exchange(ep_count, capacity, small, large):
+    (rows, heads, write, read, ogate, proj, gate, up, down, sgate, sup, sdown) = large
     half = ep_count // 2
     tok, width = rows.shape
     bf16, f32 = jnp.bfloat16, jnp.float32
     cap = capacity
-    mix_block = mix_term.shape[1]
+    tok_m, chans = heads.shape
+    state = write.shape[1]
+    mix_block = tok_m // 4
     count = len(message_names(half))
+    rounds = (ep_count - 1).bit_length()
     shapes = [
         ((tok, width), bf16),
-        (mix_term.shape, bf16),
+        ((4, mix_block, width), bf16),
+        (heads.shape, bf16),
+        (write.shape, bf16),
+        (read.shape, bf16),
+        (ogate.shape, bf16),
+        (proj.shape, bf16),
+        ((16, chans), bf16),
+        ((16, state), bf16),
+        ((16, state), bf16),
+        ((tok_m + 8, chans), f32),
+        ((tok_m + 8, state), f32),
+        ((tok_m + 8, state), f32),
+        ((tok_m, chans), f32),
+        ((tok_m, chans), f32),
+        ((tok_m, state), bf16),
+        ((tok_m, chans), f32),
+        ((state, chans), f32),
+        ((8, chans), f32),
+        ((state, chans), f32),
+        ((8, chans), f32),
+        ((rounds, state, chans), bf16),
+        ((rounds, 8, chans), f32),
+        ((rounds, state, chans), bf16),
+        ((rounds, 8, chans), f32),
         (gate.shape, bf16),
         (up.shape, bf16),
         (down.shape, bf16),
@@ -700,19 +927,19 @@
             jax.ShapeDtypeStruct((mix_block, width), bf16),
             jax.ShapeDtypeStruct((tok, width), bf16),
         ),
-        in_specs=[any_spec, vmem_spec, vmem_spec] + [any_spec] * 7,
+        in_specs=[any_spec] + [vmem_spec] * 2 + [any_spec] * 5 + [vmem_spec] * 7 + [any_spec] * 6,
         out_specs=(vmem_spec, vmem_spec),
         scratch_shapes=[pltpu.VMEM(shape, dtype) for shape, dtype in shapes]
         + [
-            pltpu.SemaphoreType.DMA((8,)),
+            pltpu.SemaphoreType.DMA((12,)),
             pltpu.SemaphoreType.DMA((count,)),
             pltpu.SemaphoreType.DMA((count,)),
         ],
         compiler_params=pltpu.CompilerParams(
-            collective_id=0, has_side_effects=True, vmem_limit_bytes=60 * 1024 * 1024
+            collective_id=0, has_side_effects=True, vmem_limit_bytes=62 * 1024 * 1024
         ),
-        name="moe_exchange",
-    )(rows, meta, gain, mix_term, gate, up, down, sgate, sup, sdown)
+        name="mixer_and_experts",
+    )(rows, *small[:2], heads, write, read, ogate, proj, *small[2:], gate, up, down, sgate, sup, sdown)
 
 
 def direct(
@@ -739,9 +966,8 @@
     shared_up_weight,
     shared_down_weight,
 ):
-    tp_count = lax.axis_size("tp")
     ep_count = lax.axis_size("ep")
-    tok_local, model_width = expert_input_rows.shape
+    tok_local = expert_input_rows.shape[0]
     experts = ep_count
     capacity = 3 * tok_local * routes.shape[1] // (2 * experts)
     score_float = router_chosen_scores.astype(jnp.float32)
@@ -754,34 +980,24 @@
     place = jnp.sum(jnp.where(choice, rank[:, :, None], 0.0), axis=0) + (routes * capacity).astype(jnp.float32)
     meta = jnp.pad(jnp.concatenate([place.T, weights.T], axis=0), ((0, 4), (0, 0)))
 
-    earlier = tail_rows_from_behind(
-        head_inputs_unfiltered, group_write_vectors, group_read_vectors, head_filter_taps.shape[0]
-    )
-    mixer_normed = mixer_rows(
-        earlier,
+    small = (
+        meta,
+        expert_norm_gain.reshape(1, -1),
+        step_preactivation,
+        extra_decay_logs,
+        head_decay_logs.reshape(-1, 1),
+        head_filter_taps,
+        write_filter_taps,
+        read_filter_taps,
+        grouped_norm_gain.reshape(1, -1),
+    )
+    large = (
+        expert_input_rows,
         head_inputs_unfiltered,
         group_write_vectors,
         group_read_vectors,
         output_gate_inputs,
-        step_preactivation,
-        extra_decay_logs,
-        head_decay_logs,
-        head_filter_taps,
-        write_filter_taps,
-        read_filter_taps,
-        grouped_norm_gain,
-    )
-    mix_block = mixer_normed.shape[0] // tp_count
-    mix_term = jnp.dot(
-        mixer_normed, mixer_output_weight, preferred_element_type=jnp.float32
-    ).astype(jnp.bfloat16).reshape(tp_count, mix_block, model_width)
-    return exchange(
-        ep_count,
-        capacity,
-        expert_input_rows,
-        meta,
-        expert_norm_gain.reshape(1, -1),
-        mix_term,
+        mixer_output_weight,
         routed_gate_weight[0],
         routed_up_weight[0],
         routed_down_weight[0],
@@ -789,6 +1005,7 @@
         shared_up_weight,
         shared_down_weight,
     )
+    return exchange(ep_count, capacity, small, large)
 
 
 def fits_direct(mesh, tok_local, top_count, local_experts):

time: 171 us -> 125 us (0.73)
  starting transfers between devices: 19.3 us -> 0 us
  matrix products: 17.7 us -> 0.13 us
  Pallas kernels: 100 us -> 115 us
  waiting for transfers between devices: 12.1 us -> 0 us
  other arithmetic: 11.2 us -> 3.37 us
  local copies, waits for them, and re-layouts: 8.42 us -> 4.78 us
    ppermute x4 -> x0, starting transfers between devices: 19.3 us -> none  [from_behind(): return lax.ppermute(value, axis, pairs)]
    dot_general x7 -> x0, matrix products: 17.6 us -> none  [the longest x1 5.58 us: mixer_rows(): jnp.einsum('gebc,cgepn->bgepn', carry_weights, block_states, precision=hi...]
    pallas_call x1, Pallas kernels: 100 us -> 115 us  [exchange(): pl.pallas_call(functools.partial(exchange_kernel, ep_count, capacity), ou...]
    ppermute x4 -> x0, waiting for transfers between devices: 12.1 us -> none  [from_behind(): return lax.ppermute(value, axis, pairs)]
    mul x6 -> x0, other arithmetic: 4.48 us -> none  [the longest x3 2.52 us: conv_silu(): weights[offset].astype(jnp.float32)]
    slice x9 -> x0, local copies, waits for them, and re-layouts: 2.41 us -> none  [the longest x1 0.74 us: tail_rows_from_behind(): read_vectors[start:]]
    unnamed x15 -> x2, local copies, waits for them, and re-layouts: 3.76 us -> 3.45 us
  transfers between devices with their start and end apart: 4 -> 0, of which waited for: 3 -> 0; matrix products, arithmetic and copies ran while one was open for 6% -> 0% of each run, Pallas kernels for 0% -> 0%
where the time goes in v2:
time: 125 us; the launch traced here: 124 us
  Pallas kernels  115 us (92%)
  local copies, waits for them, and re-layouts  4.78 us (4%)
  other arithmetic  3.37 us (3%)
    pallas_call x1, Pallas kernels, exchange(): pl.pallas_call(functools.partial(exchange_kernel, ep_count, capacity), ou...  115 us
    unnamed x2, local copies, waits for them, and re-layouts  3.45 us

profile of v2, /device:TPU:0, one launch (start us, length us, event | category | flops | bytes accessed | tf_op | source)
XLA Modules:
  0.0 123.8 jit_solution(17690393783838174644)
XLA Ops:
  0.6 0.7 convert_reduce_fusion
  1.3 0.7 fusion.1
  2.0 0.1 fusion
  2.1 0.7 select_reduce_fusion
  2.8 0.7 fusion.3
  3.5 0.6 select_maximum_fusion.meta_ref
  4.1 1.3 %copy.26.decay_ref = f32[16,1]{1,0:T(8,128)} copy(f32[16,1]{0,1:T(1,128)} %bitcast.16) | data formatting | bytes 128 | tf_op jit(solution)/shard_map/reshape | solution.py:988
  5.5 114.9 %mixer_and_experts.1 = (bf16[32,2048]{1,0:T(8,128)(2,1)}, bf16[128,2048]{1,0:T(8,128)(2,1)}) custom-call(bf16[128,2048]{1,0:T(8,128)(2,1)} %rows_hbm.1, f32[8,128]{1,0:T(8,128)} %select_maximum_fusion.meta_ref, f32[1,2048]{1,0:T(1,128)} %bitcast.14, bf16[128,1024]{1,0:T(8,128)(2,1)} %heads_hbm.1, bf16[128,128]{1,0:T(8,128)(2,1)} %write_hbm.1, ...), custom_call_target="tpu_custom_call" | custom-call | tf_op jit(solution)/shard_map/mixer_and_experts/pallas_call | solution.py:924
  120.4 1.6 %copy.29 = bf16[32,2048]{1,0:T(8,128)(2,1)} copy(bf16[32,2048]{1,0:T(8,128)(2,1)} %get-tuple-element.6) | data formatting | bytes 262144
  122.0 1.9 %copy.30 = bf16[128,2048]{1,0:T(8,128)(2,1)} copy(bf16[128,2048]{1,0:T(8,128)(2,1)} %get-tuple-element.7) | data formatting | bytes 1048576

commit v3 on v2

--- a/solution.py
+++ b/solution.py
@@ -300,26 +300,33 @@
 
 
 def message_names(half):
-    names = ["meta_core", "meta_y", "meta_far", "rows_core", "rows_y", "rows_fwd", "shared", "dense", "mix_core", "mix_far", "mix_y"]
-    names += ["halo_h", "halo_w", "halo_r"]
-    for r in range((2 * half - 1).bit_length()):
-        names += [f"state{r}", f"decay{r}"]
+    names = ["meta_y", "rows_y", "dense", "mix_core", "mix_far", "mix_y", "halo_h", "halo_w", "halo_r"]
+    names += ["gate", "up", "down", "sgate", "sup", "sdown"]
+    names += ["pair_s", "pair_d", "plane_s", "plane_d", "last_s"]
     for d in range(half):
-        names += [f"{kind}{d}" for kind in ("a", "ay", "ac", "ra", "ry", "fa", "b", "bc", "rb", "fb")]
+        names += [f"{kind}{d}" for kind in ("a", "ay", "ry", "fa", "bo", "by", "fb")]
     return {name: i for i, name in enumerate(names)}
 
 
 def exchange_kernel(
     ep_count,
     capacity,
+    order,
     rows_hbm,
-    meta_ref,
-    gain_ref,
     heads_hbm,
     write_hbm,
     read_hbm,
     ogate_hbm,
     proj_hbm,
+    gate_hbm,
+    up_hbm,
+    down_hbm,
+    sgate_hbm,
+    sup_hbm,
+    sdown_hbm,
+    routes_ref,
+    scores_ref,
+    gain_ref,
     step_ref,
     extra_ref,
     decay_ref,
@@ -327,21 +334,20 @@
     wtaps_ref,
     rtaps_ref,
     mgain_ref,
-    gate_hbm,
-    up_hbm,
-    down_hbm,
-    sgate_hbm,
-    sup_hbm,
-    sdown_hbm,
     mix_out,
     moe_out,
     rows_v,
-    mix_v,
     heads_v,
     write_v,
     read_v,
     ogate_v,
     proj_v,
+    gate_v,
+    up_v,
+    down_v,
+    sgate_v,
+    sup_v,
+    sdown_v,
     halo_h,
     halo_w,
     halo_r,
@@ -354,18 +360,17 @@
     grow_v,
     own_s,
     own_d,
+    plane_s,
+    plane_d,
     bef_s,
-    bef_d,
     out_s,
     out_d,
     in_s,
     in_d,
-    gate_v,
-    up_v,
-    down_v,
-    sgate_v,
-    sup_v,
-    sdown_v,
+    mix_v,
+    mix_r,
+    mix_s,
+    mix_ry,
     meta_v,
     grp,
     pack_a,
@@ -374,26 +379,18 @@
     xb,
     ya,
     yb,
-    ra,
-    rb,
-    sa,
-    sb,
     ry,
     fa,
     ret_a,
     ret_b,
-    sp,
-    rsp,
     dense,
     dense_s,
     dense_r,
-    mix_r,
-    mix_s,
-    mix_ry,
     load_sem,
     send_sem,
     recv_sem,
 ):
+    f32, bf16 = jnp.float32, jnp.bfloat16
     half = ep_count // 2
     cap = capacity
     tok, width = rows_v.shape
@@ -410,7 +407,7 @@
     t_core = t + 1 - 2 * (t % 2)
     t_y = (t + 2) % 4
     t_far = (t_core + 2) % 4
-    core, ydev, far = (e, t_core), (e, t_y), (e, t_far)
+    core, ydev = (e, t_core), (e, t_y)
 
     def to_a(d):
         return (other + (q + d) % half, t)
@@ -428,15 +425,15 @@
     for i, (name, src, dst) in enumerate(
         (
             ("rows", rows_hbm, rows_v),
-            ("sgate", sgate_hbm, sgate_v),
-            ("sup", sup_hbm, sup_v),
-            ("sdown", sdown_hbm, sdown_v),
-            ("gate", gate_hbm, gate_v),
-            ("up", up_hbm, up_v),
-            ("down", down_hbm, down_v),
             ("heads", heads_hbm, heads_v),
             ("write", write_hbm, write_v),
             ("read", read_hbm, read_v),
+            ("sgate", sgate_hbm, sgate_v.at[0]),
+            ("sup", sup_hbm, sup_v.at[0]),
+            ("sdown", sdown_hbm, sdown_v.at[0]),
+            ("gate", gate_hbm, gate_v.at[0]),
+            ("up", up_hbm, up_v.at[0]),
+            ("down", down_hbm, down_v.at[0]),
             ("ogate", ogate_hbm, ogate_v),
             ("proj", proj_hbm, proj_v),
         )
@@ -464,133 +461,157 @@
     def arrived(name):
         copies[name].wait_recv()
 
+    guarded = []
+
+    def send_if(name, src, dst, device, here):
+        prepare(name, src, dst, device)
+        guarded.append((name, here))
+
+        @pl.when(here)
+        def _():
+            copies[name].start()
+
     barrier = pltpu.get_barrier_semaphore()
-    peers = [core, ydev, far] + [to_a(d) for d in range(half)] + [to_b(d) for d in range(1, half)]
+    peers = [core, ydev] + [to_a(d) for d in range(half)] + [to_b(d) for d in range(1, half)]
     for peer in peers:
         pl.semaphore_signal(barrier, inc=1, device_id=peer, device_id_type=MESH)
 
-    meta_v[0] = meta_ref[...]
-    f32, bf16 = jnp.float32, jnp.bfloat16
+    row = lax.broadcasted_iota(jnp.int32, (tok, tok), 0)
+    lane = lax.broadcasted_iota(jnp.int32, (tok, tok), 1)
+    routed = [routes_ref[k : k + 1, :] for k in range(2)]
+    expert_row = lax.broadcasted_iota(jnp.int32, (ep_count, tok), 0)
+    chosen = [routed[k] == expert_row for k in range(2)]
+    named = jnp.where(chosen[0] | chosen[1], 1.0, 0.0).astype(bf16)
+    rank = jnp.dot(
+        named, jnp.where(row < lane, 1.0, 0.0).astype(bf16), preferred_element_type=f32
+    )
+    scores = scores_ref[...].astype(f32)
+    total_score = jnp.sum(scores, axis=0, keepdims=True)
+    meta_v[0] = jnp.zeros(meta_v.shape[1:], f32)
+    for k in range(2):
+        meta_v[0, k : k + 1, :] = jnp.sum(
+            jnp.where(chosen[k], rank, 0.0), axis=0, keepdims=True
+        ) + (routed[k] * cap).astype(f32)
+        meta_v[0, 2 + k : 3 + k, :] = scores[k : k + 1, :] / total_score * route_scale
+
     loads["rows"].wait()
 
     def norm_rows(i, carry):
         at = pl.ds(pl.multiple_of(i * 16, 16), 16)
-        x = rows_v[at, :].astype(jnp.float32)
+        x = rows_v[at, :].astype(f32)
         scale = lax.rsqrt(jnp.mean(x * x, axis=-1, keepdims=True) + eps_norm)
-        grp[0, at, :] = (x * scale * gain_ref[...]).astype(jnp.bfloat16)
+        grp[0, at, :] = (x * scale * gain_ref[...]).astype(bf16)
         return carry
 
     lax.fori_loop(0, tok // 16, norm_rows, 0)
     pl.semaphore_wait(barrier, len(peers))
 
-    send("meta_y", meta_v.at[0], meta_v.at[1], ydev)
-    send("meta_core", meta_v.at[0], meta_v.at[2], core)
-    send("meta_far", meta_v.at[0], meta_v.at[3], far)
-    send("rows_y", grp.at[0], grp.at[1], ydev)
-    send("rows_core", grp.at[0], grp.at[2], core)
-
-
-    nxt = ((e + 1) % ep_count, t)
-    halo_rows = halo_h.shape[0]
-    tail = pl.ds(tok_m - halo_rows, halo_rows)
-    for name in ("heads", "write", "read"):
-        loads[name].wait()
-    send("halo_h", heads_v.at[tail], halo_h, nxt)
-    send("halo_w", write_v.at[tail], halo_w, nxt)
-    send("halo_r", read_v.at[tail], halo_r, nxt)
-
-    def pack(pos, expert, put):
-        places = lax.broadcasted_iota(jnp.int32, (cap, tok), 0) + expert * cap
-        places = places.astype(jnp.float32)
-        chosen = (places == meta_v[pos, 0:1, :]) | (places == meta_v[pos, 1:2, :])
-        chosen = jnp.where(chosen, 1.0, 0.0).astype(jnp.bfloat16)
+    def pack(pos, expert_at, ref, lead, low):
+        places = lax.broadcasted_iota(jnp.int32, (cap, tok), 0) + expert_at * cap
+        places = places.astype(f32)
+        picked = (places == meta_v[pos, 0:1, :]) | (places == meta_v[pos, 1:2, :])
+        picked = jnp.where(picked, 1.0, 0.0).astype(bf16)
         for n in range(0, width, col):
+            ref[lead, low : low + cap, n : n + col] = jnp.dot(
+                picked, grp[pos, :, n : n + col], preferred_element_type=f32
+            ).astype(bf16)
+
+    def rows_out():
+        send("meta_y", meta_v.at[0], meta_v.at[1], ydev)
+        send("rows_y", grp.at[0], grp.at[1], ydev)
+
+    def halo_out():
+        following = ((e + 1) % ep_count, t)
+        kept = halo_h.shape[0]
+        tail = pl.ds(tok_m - kept, kept)
+        for name in ("heads", "write", "read"):
+            loads[name].wait()
+        send("halo_h", heads_v.at[tail], halo_h, following)
+        send("halo_w", write_v.at[tail], halo_w, following)
+        send("halo_r", read_v.at[tail], halo_r, following)
+
+    def weights_out():
+        send("sgate", sgate_hbm, sgate_v.at[1], core)
+        send("sup", sup_hbm, sup_v.at[1], core)
+        send("sdown", sdown_hbm, sdown_v.at[1], core)
+        send("gate", gate_hbm, gate_v.at[1], core)
+        send("up", up_hbm, up_v.at[1], core)
+        send("down", down_hbm, down_v.at[1], core)
+
+    def weights_in(names):
+        for name in names:
+            loads[name].wait()
+            arrived(name)
+
+    def gated_product(x, first_v, second_v, third_v, put):
+        hidden = []
+        for s in range(2):
+            g = jnp.dot(x, first_v[s], preferred_element_type=f32)
+            u = jnp.dot(x, second_v[s], preferred_element_type=f32)
+            hidden.append((jax.nn.silu(g) * u).astype(bf16))
+        for n in range(0, width, col):
+            at = slice(n, n + col)
             put(
-                n,
-                jnp.dot(chosen, grp[pos, :, n : n + col], preferred_element_type=jnp.float32).astype(
-                    jnp.bfloat16
-                ),
+                at,
+                jnp.dot(hidden[0], third_v[0, :, at], preferred_element_type=f32)
+                + jnp.dot(hidden[1], third_v[1, :, at], preferred_element_type=f32),
             )
 
-    def put_in(ref, *lead):
-        def put(n, value):
-            ref[(*lead, slice(n, n + col))] = value
-
-        return put
-
-    for d in range(half):
-        pack(0, other + (q + d) % half, put_in(pack_a, d, slice(None)))
+    def shared_rows(pos):
+        def put(at, value):
+            dense[pos, :, at] = value
+
+        gated_product(grp[pos], sgate_v, sup_v, sdown_v, put)
+
+    def a0(d):
+        pack(0, other + (q + d) % half, pack_a, d, 0)
         send(f"a{d}", pack_a.at[d], xa.at[d, pl.ds(0, cap)], to_a(d))
-
-    def shared_rows(pos):
-        x = grp[pos]
-        g = jnp.dot(x, sgate_v[...], preferred_element_type=jnp.float32)
-        u = jnp.dot(x, sup_v[...], preferred_element_type=jnp.float32)
-        h = (jax.nn.silu(g) * u).astype(jnp.bfloat16)
-        for n in range(0, width, col):
-            sp[pos, :, n : n + col] = jnp.dot(
-                h, sdown_v[:, n : n + col], preferred_element_type=jnp.float32
-            ).astype(jnp.bfloat16)
-
-    def expert(x_ref, y_ref):
-        x = x_ref[...]
-        g = jnp.dot(x, gate_v[...], preferred_element_type=jnp.float32)
-        u = jnp.dot(x, up_v[...], preferred_element_type=jnp.float32)
-        h = (jax.nn.silu(g) * u).astype(jnp.bfloat16)
-        for n in range(0, width, col):
-            y_ref[:, n : n + col] = jnp.dot(
-                h, down_v[:, n : n + col], preferred_element_type=jnp.float32
-            ).astype(jnp.bfloat16)
 
     def a1(d):
         arrived(f"a{d}")
         send(f"ay{d}", xa.at[d, pl.ds(0, cap)], xa.at[d, pl.ds(cap, cap)], ydev)
 
-    def a2(d):
+    def a3(d):
         arrived(f"ay{d}")
-        send(f"ac{d}", xa.at[d, pl.ds(0, 2 * cap)], xa.at[d, pl.ds(2 * cap, 2 * cap)], core)
-
-    def a3(d):
-        arrived(f"ac{d}")
-        expert(xa.at[d], ya.at[d])
-        send(f"ra{d}", ya.at[d, pl.ds(2 * cap, 2 * cap)], ra.at[d], core)
-
-    def a4(d):
-        arrived(f"ra{d}")
-        sa[d] = (ya[d, 0 : 2 * cap].astype(f32) + ra[d].astype(f32)).astype(jnp.bfloat16)
-        send(f"ry{d}", sa.at[d, pl.ds(cap, cap)], ry.at[d], ydev)
+
+        def put(at, value):
+            ya[d, :, at] = value.astype(bf16)
+
+        gated_product(xa[d], gate_v, up_v, down_v, put)
+        send(f"ry{d}", ya.at[d, pl.ds(cap, cap)], ry.at[d], ydev)
 
     def a5(d):
         arrived(f"ry{d}")
-        fa[d] = (sa[d, 0:cap].astype(f32) + ry[d].astype(f32)).astype(jnp.bfloat16)
+        fa[d] = (ya[d, 0:cap].astype(f32) + ry[d].astype(f32)).astype(bf16)
         send(f"fa{d}", fa.at[d], ret_a.at[pl.ds(d * cap, cap)], from_a(d))
 
-    def b1(d):
-        for p in range(2):
-            pack(p, base + (q + d) % half, put_in(pack_b, d - 1, slice(p * cap, (p + 1) * cap)))
-        send(f"b{d}", pack_b.at[d - 1], xb.at[d, pl.ds(0, 2 * cap)], to_b(d))
-
-    def b2(d):
-        arrived(f"b{d}")
-        send(f"bc{d}", xb.at[d, pl.ds(0, 2 * cap)], xb.at[d, pl.ds(2 * cap, 2 * cap)], core)
+    def bo(d):
+        pack(0, base + (q + d) % half, pack_b, d - 1, 0)
+        send(f"bo{d}", pack_b.at[d - 1, pl.ds(0, cap)], xb.at[d, pl.ds(0, cap)], to_b(d))
+
+    def by(d):
+        pack(1, base + (q + d) % half, pack_b, d - 1, cap)
+        send(f"by{d}", pack_b.at[d - 1, pl.ds(cap, cap)], xb.at[d, pl.ds(cap, cap)], to_b(d))
 
     def b3(d):
         if d:
-            arrived(f"bc{d}")
-        expert(xb.at[d], yb.at[d])
-        send(f"rb{d}", yb.at[d, pl.ds(2 * cap, 2 * cap)], rb.at[d], core)
-
-    def b4(d):
-        arrived(f"rb{d}")
-        for p in range(2):
-            at = slice(p * cap, (p + 1) * cap)
-            total = (yb[d, at].astype(f32) + rb[d, at].astype(f32)).astype(jnp.bfloat16)
-            if d:
-                sb[d - 1, p] = total
-            else:
-                ret_b[p, 0:cap] = total
+            arrived(f"bo{d}")
+            arrived(f"by{d}")
+        else:
+            pack(0, e, xb, 0, 0)
+            pack(1, e, xb, 0, cap)
+
+        def put(at, value):
+            for p in range(2):
+                part = value[p * cap : (p + 1) * cap].astype(bf16)
+                if d:
+                    yb[d - 1, p, :, at] = part
+                else:
+                    ret_b[p, 0:cap, at] = part
+
+        gated_product(xb[d], gate_v, up_v, down_v, put)
         if d:
-            send(f"fb{d}", sb.at[d - 1], ret_b.at[:, pl.ds(d * cap, cap)], from_b(d))
+            send(f"fb{d}", yb.at[d - 1], ret_b.at[:, pl.ds(d * cap, cap)], from_b(d))
 
     def chosen_slots(columns, first):
         lanes = lax.broadcasted_iota(jnp.int32, (1, half * cap), 1)
@@ -599,7 +620,7 @@
             moved = (first + (q + d) % half - d) * cap
             code = jnp.where(lanes >= d * cap, lanes + moved, code)
         code = code.astype(f32)
-        return [jnp.where(columns[:, k : k + 1] == code, 1.0, 0.0).astype(jnp.bfloat16) for k in range(2)]
+        return [jnp.where(columns[:, k : k + 1] == code, 1.0, 0.0).astype(bf16) for k in range(2)]
 
     def mixed(columns, picks, returned):
         total = None
@@ -613,16 +634,18 @@
         picks = chosen_slots(columns, base)
         for n in range(0, width, col):
             at = slice(n, n + col)
-            value = (
-                mixed(columns, picks, ret_b[p, :, at])
-                + sp[p, :, at].astype(f32)
-                + rsp[p, :, at].astype(f32)
-            )
+            value = mixed(columns, picks, ret_b[p, :, at]) + dense[p, :, at]
             if p:
-                dense_s[:, at] = value.astype(jnp.bfloat16)
+                dense_s[:, at] = value.astype(bf16)
             else:
-                dense[:, at] = value
-
+                dense[0, :, at] = value
+
+    def dense_out():
+        for d in range(1, half):
+            arrived(f"fb{d}")
+        dense_rows(1)
+        send("dense", dense_s, dense_r, ydev)
+        dense_rows(0)
 
     def conv(x_v, halo, ext, taps_ref, n, size):
         at = slice(n, n + size)
@@ -652,7 +675,9 @@
             total = add if total is None else total + add
         return total
 
-    def mixer_local():
+    local = {}
+
+    def mixer_states():
         for name in ("halo_h", "halo_w", "halo_r"):
             arrived(name)
         for n in range(0, chans, 256):
@@ -662,9 +687,12 @@
         read = conv(read_v, halo_r, ext_r, rtaps_ref, 0, states)
         read_b[...] = read.astype(bf16)
         step = jax.nn.softplus(step_ref[...])
-        rate = step * -jnp.exp(decay_ref[...]) + extra_ref[...]
-        row = lax.broadcasted_iota(jnp.int32, (tok_m, tok_m), 0)
-        lane = lax.broadcasted_iota(jnp.int32, (tok_m, tok_m), 1)
+        square_row = lax.broadcasted_iota(jnp.int32, (heads, heads), 0)
+        square_lane = lax.broadcasted_iota(jnp.int32, (heads, heads), 1)
+        speed = jnp.sum(
+            jnp.where(square_row == square_lane, jnp.exp(decay_ref[...]), 0.0), axis=1, keepdims=True
+        )
+        rate = step * -speed + extra_ref[...]
         upto = jnp.where(row <= lane, 1.0, 0.0).astype(f32)
         cum = jnp.dot(rate, upto, precision=highest, preferred_element_type=f32)
         cum_t = jnp.transpose(cum)
@@ -674,11 +702,12 @@
         )
         weights = spread(jnp.transpose(to_end), 2)
         weighted = (hval[...] * weights).astype(bf16)
-        own_s[...] = jnp.dot(
-            jnp.transpose(write).astype(bf16), weighted, preferred_element_type=f32
-        )
-        own_d[...] = jnp.broadcast_to(spread(cum_t[tok_m - 8 : tok_m], 3)[7:8], own_d.shape)
-        state_send(0)
+        own_s[...] = jnp.dot(jnp.transpose(write).astype(bf16), weighted, preferred_element_type=f32)
+        own_d[...] = spread(cum_t[tok_m - 8 : tok_m], 3)[7:8]
+        local.update(cum=cum, cum_t=cum_t, step=step, affinity=affinity)
+
+    def mixer_rows_local():
+        cum, cum_t, step, affinity = (local[k] for k in ("cum", "cum_t", "step", "affinity"))
         grow_v[...] = spread(jnp.exp(cum_t), 2)
         causal = row >= lane
         for pair in range(heads // 2):
@@ -694,48 +723,84 @@
                 parts[0], jnp.where(side, both, zero), preferred_element_type=f32
             ) + jnp.dot(parts[1], jnp.where(side, zero, both), preferred_element_type=f32)
 
-    rounds = (ep_count - 1).bit_length()
-
-    def state_send(r):
-        by = 2**r
-        if r == 0:
-            out_s[r] = own_s[...].astype(bf16)
-            out_d[r] = own_d[...]
-        else:
-            grown = jnp.exp(own_d[0:1, :])
-            out_s[r] = (own_s[...] + grown * bef_s[...]).astype(bf16)
-            out_d[r] = own_d[...] + bef_d[...]
-
-        later = ((e + by) % ep_count, t)
-        prepare(f"state{r}", out_s.at[r], in_s.at[r], later)
-        prepare(f"decay{r}", out_d.at[r], in_d.at[r], later)
-
-        @pl.when(e + by < ep_count)
+    side_x, plane, planes = e % 2, e // 2, ep_count // 2
+    is_head = side_x == 1 - t % 2
+    is_tail = side_x == t % 2
+    later_head = is_head & (side_x == 1)
+    early_head = is_head & (side_x == 0)
+    beside = (e + 1 - 2 * side_x, t)
+    above = ((e + 2) % ep_count, t)
+
+    def states_pair():
+        @pl.when(is_tail)
         def _():
-            copies[f"state{r}"].start()
-            copies[f"decay{r}"].start()
-
-    def state_arrive(r):
-        by = 2**r
-
-        @pl.when(e < by)
+            out_s[0] = own_s[...].astype(bf16)
+            out_d[0] = own_d[...]
+
+        send_if("pair_s", out_s.at[0], in_s.at[0], beside, is_tail)
+        send_if("pair_d", out_d.at[0], in_d.at[0], beside, is_tail)
+
+    def states_plane():
+        prepare("plane_s", out_s.at[1], in_s.at[1], above)
+        prepare("plane_d", out_d.at[1], in_d.at[1], above)
+        guarded.append(("plane_s", is_head & (plane < planes - 1)))
+        guarded.append(("plane_d", is_head & (plane < planes - 1)))
+
+        @pl.when(is_head)
         def _():
-            in_s[r] = jnp.zeros(in_s.shape[1:], bf16)
-            in_d[r] = jnp.zeros(in_d.shape[1:], f32)
-
-        @pl.when(e >= by)
+            arrived("pair_s")
+            arrived("pair_d")
+
+        @pl.when(later_head)
         def _():
-            arrived(f"state{r}")
-            arrived(f"decay{r}")
-
-        if r == 0:
-            bef_s[...] = in_s[0].astype(f32)
-            bef_d[...] = in_d[0]
-        else:
-            bef_s[...] = bef_s[...] + jnp.exp(bef_d[0:1, :]) * in_s[r].astype(f32)
-            bef_d[...] = bef_d[...] + in_d[r]
-        if r + 1 < rounds:
-            state_send(r + 1)
+            plane_s[...] = own_s[...] + jnp.exp(own_d[...]) * in_s[0].astype(f32)
+
+        @pl.when(early_head)
+        def _():
+            plane_s[...] = in_s[0].astype(f32) + jnp.exp(in_d[0]) * own_s[...]
+
+        @pl.when(is_head)
+        def _():
+            plane_d[...] = own_d[...] + in_d[0]
+
+        @pl.when(is_head & (plane == 0))
+        def _():
+            in_s[1] = jnp.zeros(in_s.shape[1:], bf16)
+            in_d[1] = jnp.zeros(in_d.shape[1:], f32)
+            out_s[1] = plane_s[...].astype(bf16)
+            out_d[1] = plane_d[...]
+            copies["plane_s"].start()
+            copies["plane_d"].start()
+
+    def states_up(k):
+        @pl.when(is_head & (plane == k))
+        def _():
+            arrived("plane_s")
+            arrived("plane_d")
+            if k < planes - 1:
+                out_s[1] = (plane_s[...] + jnp.exp(plane_d[...]) * in_s[1].astype(f32)).astype(bf16)
+                out_d[1] = plane_d[...] + in_d[1]
+                copies["plane_s"].start()
+                copies["plane_d"].start()
+
+    def states_last():
+        @pl.when(later_head)
+        def _():
+            bef_s[...] = in_s[0].astype(f32) + jnp.exp(in_d[0]) * in_s[1].astype(f32)
+            out_s[2] = in_s[1]
+
+        @pl.when(early_head)
+        def _():
+            bef_s[...] = in_s[1].astype(f32)
+            out_s[2] = (own_s[...] + jnp.exp(own_d[...]) * in_s[1].astype(f32)).astype(bf16)
+
+        send_if("last_s", out_s.at[2], in_s.at[2], beside, is_head)
+
+    def states_in():
+        @pl.when(is_tail)
+        def _():
+            arrived("last_s")
+            bef_s[...] = in_s[2].astype(f32)
 
     def mixer_finish():
         square = jnp.zeros((tok_m, 1), f32)
@@ -755,81 +820,45 @@
         send("mix_core", mix_v.at[t_core], mix_r.at[0], core)
         send("mix_far", mix_v.at[t_far], mix_r.at[1], core)
 
-    loads["sgate"].wait()
-    loads["sup"].wait()
-    loads["sdown"].wait()
-    shared_rows(0)
-    mixer_local()
-    arrived("meta_y")
-    arrived("rows_y")
-    send("rows_fwd", grp.at[1], grp.at[3], core)
-    for d in range(1, half):
-        b1(d)
-    arrived("meta_core")
-    arrived("meta_far")
-    arrived("rows_core")
-    a1(0)
-    shared_rows(1)
-    shared_rows(2)
-    for p in (0, 1, 2):
-        pack(p, e, put_in(xb, 0, slice(p * cap, (p + 1) * cap)))
-    arrived("rows_fwd")
-    shared_rows(3)
-    send("shared", sp.at[pl.ds(2, 2)], rsp, core)
-    pack(3, e, put_in(xb, 0, slice(3 * cap, 4 * cap)))
-    a2(0)
-    loads["gate"].wait()
-    loads["up"].wait()
-    loads["down"].wait()
-    b3(0)
-    state_arrive(0)
-    a3(0)
-    a1(1)
-    b2(1)
-    b4(0)
-    a4(0)
-    b3(1)
-    a2(1)
-    b4(1)
-    b2(2)
-    a3(1)
-    a5(0)
-    state_arrive(1)
-    a1(2)
-    a4(1)
-    b3(2)
-    a2(2)
-    b4(2)
-    b2(3)
-    a3(2)
-    a5(1)
-    a1(3)
-    a4(2)
-    b3(3)
-    a2(3)
-    b4(3)
-    state_arrive(2)
-    a3(3)
-    a5(2)
-    loads["ogate"].wait()
-    loads["proj"].wait()
-    mixer_finish()
-    a4(3)
-    a5(3)
-    arrived("mix_core")
-    arrived("mix_far")
-    mix_s[...] = (mix_v[t_y].astype(f32) + mix_r[1].astype(f32)).astype(jnp.bfloat16)
-    send("mix_y", mix_s, mix_ry, ydev)
-    for d in range(1, half):
-        arrived(f"fb{d}")
-    arrived("shared")
-    dense_rows(1)
-    send("dense", dense_s, dense_r, ydev)
-    dense_rows(0)
+    def mix_across():
+        arrived("mix_core")
+        arrived("mix_far")
+        mix_s[...] = (mix_v[t_y].astype(f32) + mix_r[1].astype(f32)).astype(bf16)
+        send("mix_y", mix_s, mix_ry, ydev)
+
+    def rows_in():
+        arrived("meta_y")
+        arrived("rows_y")
+
+    steps = {
+        "rows_out": rows_out,
+        "halo_out": halo_out,
+        "weights_out": weights_out,
+        "shared_in": lambda: weights_in(("sgate", "sup", "sdown")),
+        "expert_in": lambda: weights_in(("gate", "up", "down")),
+        "mix_in": lambda: [loads[name].wait() for name in ("ogate", "proj")],
+        "rows_in": rows_in,
+        "states": mixer_states,
+        "local": mixer_rows_local,
+        "pair": states_pair,
+        "plane": states_plane,
+        "last": states_last,
+        "before": states_in,
+        "finish": mixer_finish,
+        "across": mix_across,
+        "dense": dense_out,
+    }
+    numbered = {"a0": a0, "a1": a1, "a3": a3, "a5": a5, "bo": bo, "by": by, "b3": b3, "up": states_up}
+    numbered["shared"] = shared_rows
+    for name in order.split():
+        if name in steps:
+            steps[name]()
+        else:
+            stem, number = name.split(":")
+            numbered[stem](int(number))
+
     arrived("mix_y")
-    mix_out[...] = (
-        mix_v[t].astype(f32) + mix_r[0].astype(f32) + mix_ry[...].astype(f32)
-    ).astype(jnp.bfloat16)
+    mix_out[...] = (mix_v[t].astype(f32) + mix_r[0].astype(f32) + mix_ry[...].astype(f32)).astype(bf16)
     for d in range(half):
         arrived(f"fa{d}")
     arrived("dense")
@@ -837,18 +866,46 @@
     picks = chosen_slots(columns, other)
     for n in range(0, width, col):
         at = slice(n, n + col)
-        value = mixed(columns, picks, ret_a[:, at]) + dense[:, at] + dense_r[:, at].astype(f32)
-        moe_out[:, at] = value.astype(jnp.bfloat16)
-    for r in range(rounds):
-
-        @pl.when(e + 2**r < ep_count)
-        def _():
-            copies[f"state{r}"].wait_send()
-            copies[f"decay{r}"].wait_send()
-
+        value = mixed(columns, picks, ret_a[:, at]) + dense[0, :, at] + dense_r[:, at].astype(f32)
+        moe_out[:, at] = value.astype(bf16)
+    for name, here in guarded:
+
+        @pl.when(here)
+        def _(name=name):
+            copies[name].wait_send()
+
+    kept_back = [name for name, _ in guarded]
     for name in copies:
-        if not name.startswith(("state", "decay")):
+        if name not in kept_back:
             copies[name].wait_send()
+
+
+def exchange_order(half):
+    before = ["rows_out", "halo_out", "a0:0"]
+    before += [f"bo:{d}" for d in range(1, half)]
+    before += ["weights_out", "states", "pair"]
+    if half > 1:
+        before += ["a0:1"]
+    before += ["plane", "local", "up:1"]
+    before += [f"a0:{d}" for d in range(2, half)]
+    after = {0: ["rows_in"] + [f"by:{d}" for d in range(1, half)]}
+    after[0] += ["shared_in", "shared:1", "shared:0", "expert_in", "b3:0"]
+    after.setdefault(1, []).extend(["up:2"])
+    for d in range(1, half):
+        after.setdefault(d, []).append(f"b3:{d}")
+    for k in range(3, half):
+        after.setdefault(k - 1, []).append(f"up:{k}")
+    after.setdefault(half - 2, []).append("last")
+    after.setdefault(half - 1, []).extend(["before", "mix_in", "finish"])
+    after[half] = ["across"]
+    after[half + 1] = ["dense"]
+    steps = list(before)
+    for at in range(half + 2):
+        for kind, lag in (("a5", 2), ("a3", 1), ("a1", 0)):
+            if 0 <= at - lag < half:
+                steps.append(f"{kind}:{at - lag}")
+        steps += after.get(at, [])
+    return " ".join(steps)
 
 
 def exchange(ep_count, capacity, small, large):
@@ -861,15 +918,9 @@
     state = write.shape[1]
     mix_block = tok_m // 4
     count = len(message_names(half))
-    rounds = (ep_count - 1).bit_length()
-    shapes = [
-        ((tok, width), bf16),
-        ((4, mix_block, width), bf16),
-        (heads.shape, bf16),
-        (write.shape, bf16),
-        (read.shape, bf16),
-        (ogate.shape, bf16),
-        (proj.shape, bf16),
+    shapes = [(array.shape, bf16) for array in (rows, heads, write, read, ogate, proj)]
+    shapes += [((2, *array.shape), bf16) for array in (gate, up, down, sgate, sup, sdown)]
+    shapes += [
         ((16, chans), bf16),
         ((16, state), bf16),
         ((16, state), bf16),
@@ -881,27 +932,22 @@
         ((tok_m, state), bf16),
         ((tok_m, chans), f32),
         ((state, chans), f32),
-        ((8, chans), f32),
+        ((1, chans), f32),
         ((state, chans), f32),
-        ((8, chans), f32),
-        ((rounds, state, chans), bf16),
-        ((rounds, 8, chans), f32),
-        ((rounds, state, chans), bf16),
-        ((rounds, 8, chans), f32),
-        (gate.shape, bf16),
-        (up.shape, bf16),
-        (down.shape, bf16),
-        (sgate.shape, bf16),
-        (sup.shape, bf16),
-        (sdown.shape, bf16),
-        ((4, 8, tok), f32),
-        ((4, tok, width), bf16),
+        ((1, chans), f32),
+        ((state, chans), f32),
+        ((3, state, chans), bf16),
+        ((2, 1, chans), f32),
+        ((3, state, chans), bf16),
+        ((2, 1, chans), f32),
+        ((4, mix_block, width), bf16),
+        ((2, mix_block, width), bf16),
+        ((mix_block, width), bf16),
+        ((mix_block, width), bf16),
+        ((2, 8, tok), f32),
+        ((2, tok, width), bf16),
         ((half, cap, width), bf16),
         ((half - 1, 2 * cap, width), bf16),
-        ((half, 4 * cap, width), bf16),
-        ((half, 4 * cap, width), bf16),
-        ((half, 4 * cap, width), bf16),
-        ((half, 4 * cap, width), bf16),
         ((half, 2 * cap, width), bf16),
         ((half, 2 * cap, width), bf16),
         ((half, 2 * cap, width), bf16),
@@ -910,28 +956,23 @@
         ((half, cap, width), bf16),
         ((half * cap, width), bf16),
         ((2, half * cap, width), bf16),
-        ((4, tok, width), bf16),
-        ((2, tok, width), bf16),
-        ((tok, width), f32),
+        ((2, tok, width), f32),
         ((tok, width), bf16),
         ((tok, width), bf16),
-        ((2, mix_block, width), bf16),
-        ((mix_block, width), bf16),
-        ((mix_block, width), bf16),
     ]
     any_spec = pl.BlockSpec(memory_space=pl.ANY)
     vmem_spec = pl.BlockSpec(memory_space=pltpu.VMEM)
     return pl.pallas_call(
-        functools.partial(exchange_kernel, ep_count, capacity),
+        functools.partial(exchange_kernel, ep_count, capacity, exchange_order(half)),
         out_shape=(
             jax.ShapeDtypeStruct((mix_block, width), bf16),
             jax.ShapeDtypeStruct((tok, width), bf16),
         ),
-        in_specs=[any_spec] + [vmem_spec] * 2 + [any_spec] * 5 + [vmem_spec] * 7 + [any_spec] * 6,
+        in_specs=[any_spec] * len(large) + [vmem_spec] * len(small),
         out_specs=(vmem_spec, vmem_spec),
         scratch_shapes=[pltpu.VMEM(shape, dtype) for shape, dtype in shapes]
         + [
-            pltpu.SemaphoreType.DMA((12,)),
+            pltpu.SemaphoreType.DMA((len(large),)),
             pltpu.SemaphoreType.DMA((count,)),
             pltpu.SemaphoreType.DMA((count,)),
         ],
@@ -939,7 +980,7 @@
             collective_id=0, has_side_effects=True, vmem_limit_bytes=62 * 1024 * 1024
         ),
         name="mixer_and_experts",
-    )(rows, *small[:2], heads, write, read, ogate, proj, *small[2:], gate, up, down, sgate, sup, sdown)
+    )(*large, *small)
 
 
 def direct(
@@ -967,25 +1008,14 @@
     shared_down_weight,
 ):
     ep_count = lax.axis_size("ep")
-    tok_local = expert_input_rows.shape[0]
-    experts = ep_count
-    capacity = 3 * tok_local * routes.shape[1] // (2 * experts)
-    score_float = router_chosen_scores.astype(jnp.float32)
-    weights = score_float / jnp.sum(score_float, axis=1, keepdims=True) * route_scale
-    choice = routes[None, :, :] == jnp.arange(experts, dtype=jnp.int32)[:, None, None]
-    named = jnp.any(choice, axis=2)
-    row_order = jnp.arange(tok_local, dtype=jnp.int32)
-    earlier_rows = (row_order[:, None] < row_order[None, :]).astype(jnp.bfloat16)
-    rank = jnp.dot(named.astype(jnp.bfloat16), earlier_rows, preferred_element_type=jnp.float32)
-    place = jnp.sum(jnp.where(choice, rank[:, :, None], 0.0), axis=0) + (routes * capacity).astype(jnp.float32)
-    meta = jnp.pad(jnp.concatenate([place.T, weights.T], axis=0), ((0, 4), (0, 0)))
-
+    capacity = 3 * expert_input_rows.shape[0] * routes.shape[1] // (2 * ep_count)
     small = (
-        meta,
+        routes.T,
+        router_chosen_scores.T,
         expert_norm_gain.reshape(1, -1),
         step_preactivation,
         extra_decay_logs,
-        head_decay_logs.reshape(-1, 1),
+        head_decay_logs.reshape(1, -1),
         head_filter_taps,
         write_filter_taps,
         read_filter_taps,
@@ -1008,18 +1038,19 @@
     return exchange(ep_count, capacity, small, large)
 
 
-def fits_direct(mesh, tok_local, top_count, local_experts):
-    ep_count = mesh.shape["ep"]
-    experts = ep_count * local_experts
+def fits_direct(mesh, rows, mix_rows, top_count, experts, groups):
+    ep_count, tp_count = mesh.shape["ep"], mesh.shape["tp"]
+    tok_local = rows // (ep_count * tp_count)
     capacity = 3 * tok_local * top_count // (2 * experts)
     return (
-        mesh.shape["tp"] == 4
-        and ep_count % 2 == 0
-        and ep_count <= 8
-        and local_experts == 1
+        tp_count == 4
+        and groups == tp_count
+        and experts == ep_count
+        and ep_count in (4, 8)
         and top_count == 2
         and capacity % 16 == 0
         and tok_local == 128
+        and mix_rows == tok_local * ep_count
     )
 
 
@@ -1050,14 +1081,20 @@
     )
     out_specs = (P(("ep", "tp"), None), P(("ep", "tp"), None))
     def step(*args):
-        devices = mesh.shape["ep"] * mesh.shape["tp"]
-        body = (
-            direct
-            if fits_direct(mesh, args[12].shape[0] // devices, args[14].shape[1], args[16].shape[0] // mesh.shape["ep"])
-            else local
+        direct_form = fits_direct(
+            mesh,
+            args[12].shape[0],
+            args[0].shape[0],
+            args[14].shape[1],
+            args[16].shape[0],
+            args[1].shape[1] // STATE,
         )
         return jax.shard_map(
-            body, mesh=mesh, in_specs=in_specs, out_specs=out_specs, check_vma=False
+            direct if direct_form else local,
+            mesh=mesh,
+            in_specs=in_specs,
+            out_specs=out_specs,
+            check_vma=False,
         )(*args)
 
     return step

time: 125 us -> 96.9 us (0.78)
  the two profiles are of different devices: /device:TPU:0 before, /device:TPU:24 now
where the time goes in v3:
time: 96.9 us; the launch traced here: 96.7 us
  Pallas kernels  92.6 us (96%)
  local copies, waits for them, and re-layouts  3.45 us (4%)
    pallas_call x1, Pallas kernels, exchange(): pl.pallas_call(functools.partial(exchange_kernel, ep_count, capacity, exc...  92.6 us
    unnamed x2, local copies, waits for them, and re-layouts  3.45 us

profile of v3, /device:TPU:24, one launch (start us, length us, event | category | flops | bytes accessed | tf_op | source)
XLA Modules:
  0.0 96.7 jit_solution(17435706776002049332)
XLA Ops:
  0.6 92.6 %mixer_and_experts.1 = (bf16[32,2048]{1,0:T(8,128)(2,1)}, bf16[128,2048]{1,0:T(8,128)(2,1)}) custom-call(bf16[128,2048]{1,0:T(8,128)(2,1)} %rows_hbm.1, bf16[128,1024]{1,0:T(8,128)(2,1)} %heads_hbm.1, bf16[128,128]{1,0:T(8,128)(2,1)} %write_hbm.1, bf16[128,128]{1,0:T(8,128)(2,1)} %read_hbm.1, bf16[128,1024]{1,0:T(8,128)(2,1)} %ogate_hbm.1, ...), custom_call_target="tpu_custom_call" | custom-call | tf_op jit(solution)/shard_map/mixer_and_experts/pallas_call | solution.py:965
  93.3 1.6 %copy.26 = bf16[32,2048]{1,0:T(8,128)(2,1)} copy(bf16[32,2048]{1,0:T(8,128)(2,1)} %get-tuple-element.4) | data formatting | bytes 262144
  94.8 1.9 %copy.27 = bf16[128,2048]{1,0:T(8,128)(2,1)} copy(bf16[128,2048]{1,0:T(8,128)(2,1)} %get-tuple-element.5) | data formatting | bytes 1048576

commit v4 on v3

--- a/solution.py
+++ b/solution.py
@@ -299,19 +299,40 @@
     return (mixer_result.astype(jnp.bfloat16), moe_total.astype(jnp.bfloat16))
 
 
-def message_names(half):
-    names = ["meta_y", "rows_y", "dense", "mix_core", "mix_far", "mix_y", "halo_h", "halo_w", "halo_r"]
-    names += ["gate", "up", "down", "sgate", "sup", "sdown"]
-    names += ["pair_s", "pair_d", "plane_s", "plane_d", "last_s"]
-    for d in range(half):
-        names += [f"{kind}{d}" for kind in ("a", "ay", "ry", "fa", "bo", "by", "fb")]
-    return {name: i for i, name in enumerate(names)}
+(
+    M_META_Y,
+    M_ROWS_Y,
+    M_DENSE,
+    M_MIX_CORE,
+    M_MIX_FAR,
+    M_MIX_Y,
+    M_HALO_H,
+    M_HALO_W,
+    M_HALO_R,
+    M_GATE,
+    M_UP,
+    M_DOWN,
+    M_SGATE,
+    M_SUP,
+    M_SDOWN,
+    M_PAIR_S,
+    M_PAIR_D,
+    M_PLANE_S,
+    M_PLANE_D,
+    M_LAST_S,
+) = range(20)
+B_A, B_AY, B_RY, B_FA, B_BO, B_BY, B_FB = range(7)
+SINGLE = 20
+BLOCK_KINDS = 7
+
+
+def block_message(kind, d):
+    return SINGLE + BLOCK_KINDS * d + kind
 
 
 def exchange_kernel(
     ep_count,
     capacity,
-    order,
     rows_hbm,
     heads_hbm,
     write_hbm,
@@ -398,7 +419,6 @@
     heads = step_ref.shape[0]
     head_dim = chans // heads
     col = 512
-    ids = message_names(half)
     e = lax.axis_index("ep")
     t = lax.axis_index("tp")
     base = (e // half) * half
@@ -421,35 +441,32 @@
     def from_b(d):
         return (base + (q + half - d) % half, t)
 
-    loads = {}
-    for i, (name, src, dst) in enumerate(
-        (
-            ("rows", rows_hbm, rows_v),
-            ("heads", heads_hbm, heads_v),
-            ("write", write_hbm, write_v),
-            ("read", read_hbm, read_v),
-            ("sgate", sgate_hbm, sgate_v.at[0]),
-            ("sup", sup_hbm, sup_v.at[0]),
-            ("sdown", sdown_hbm, sdown_v.at[0]),
-            ("gate", gate_hbm, gate_v.at[0]),
-            ("up", up_hbm, up_v.at[0]),
-            ("down", down_hbm, down_v.at[0]),
-            ("ogate", ogate_hbm, ogate_v),
-            ("proj", proj_hbm, proj_v),
-        )
+    loads = []
+    for src, dst in (
+        (rows_hbm, rows_v),
+        (heads_hbm, heads_v),
+        (write_hbm, write_v),
+        (read_hbm, read_v),
+        (sgate_hbm, sgate_v.at[0]),
+        (sup_hbm, sup_v.at[0]),
+        (sdown_hbm, sdown_v.at[0]),
+        (gate_hbm, gate_v.at[0]),
+        (up_hbm, up_v.at[0]),
+        (down_hbm, down_v.at[0]),
+        (ogate_hbm, ogate_v),
+        (proj_hbm, proj_v),
     ):
-        loads[name] = pltpu.make_async_copy(src, dst, load_sem.at[i])
-        loads[name].start()
+        loads.append(pltpu.make_async_copy(src, dst, load_sem.at[len(loads)]))
+        loads[-1].start()
 
     copies = {}
 
     def prepare(name, src, dst, device):
-        i = ids[name]
         copies[name] = pltpu.make_async_remote_copy(
             src_ref=src,
             dst_ref=dst,
-            send_sem=send_sem.at[i],
-            recv_sem=recv_sem.at[i],
+            send_sem=send_sem.at[name],
+            recv_sem=recv_sem.at[name],
             device_id=device,
             device_id_type=MESH,
         )
@@ -494,7 +511,7 @@
         ) + (routed[k] * cap).astype(f32)
         meta_v[0, 2 + k : 3 + k, :] = scores[k : k + 1, :] / total_score * route_scale
 
-    loads["rows"].wait()
+    loads[0].wait()
 
     def norm_rows(i, carry):
         at = pl.ds(pl.multiple_of(i * 16, 16), 16)
@@ -517,31 +534,40 @@
             ).astype(bf16)
 
     def rows_out():
-        send("meta_y", meta_v.at[0], meta_v.at[1], ydev)
-        send("rows_y", grp.at[0], grp.at[1], ydev)
+        send(M_META_Y, meta_v.at[0], meta_v.at[1], ydev)
+        send(M_ROWS_Y, grp.at[0], grp.at[1], ydev)
 
     def halo_out():
         following = ((e + 1) % ep_count, t)
         kept = halo_h.shape[0]
         tail = pl.ds(tok_m - kept, kept)
-        for name in ("heads", "write", "read"):
-            loads[name].wait()
-        send("halo_h", heads_v.at[tail], halo_h, following)
-        send("halo_w", write_v.at[tail], halo_w, following)
-        send("halo_r", read_v.at[tail], halo_r, following)
+        for load in loads[1:4]:
+            load.wait()
+        send(M_HALO_H, heads_v.at[tail], halo_h, following)
+        send(M_HALO_W, write_v.at[tail], halo_w, following)
+        send(M_HALO_R, read_v.at[tail], halo_r, following)
 
     def weights_out():
-        send("sgate", sgate_hbm, sgate_v.at[1], core)
-        send("sup", sup_hbm, sup_v.at[1], core)
-        send("sdown", sdown_hbm, sdown_v.at[1], core)
-        send("gate", gate_hbm, gate_v.at[1], core)
-        send("up", up_hbm, up_v.at[1], core)
-        send("down", down_hbm, down_v.at[1], core)
-
-    def weights_in(names):
-        for name in names:
-            loads[name].wait()
+        send(M_SGATE, sgate_hbm, sgate_v.at[1], core)
+        send(M_SUP, sup_hbm, sup_v.at[1], core)
+        send(M_SDOWN, sdown_hbm, sdown_v.at[1], core)
+        send(M_GATE, gate_hbm, gate_v.at[1], core)
+        send(M_UP, up_hbm, up_v.at[1], core)
+        send(M_DOWN, down_hbm, down_v.at[1], core)
+
+    def shared_in():
+        for load, name in zip(loads[4:7], (M_SGATE, M_SUP, M_SDOWN)):
+            load.wait()
             arrived(name)
+
+    def expert_in():
+        for load, name in zip(loads[7:10], (M_GATE, M_UP, M_DOWN)):
+            load.wait()
+            arrived(name)
+
+    def mix_in():
+        for load in loads[10:12]:
+            load.wait()
 
     def gated_product(x, first_v, second_v, third_v, put):
         hidden = []
@@ -565,38 +591,38 @@
 
     def a0(d):
         pack(0, other + (q + d) % half, pack_a, d, 0)
-        send(f"a{d}", pack_a.at[d], xa.at[d, pl.ds(0, cap)], to_a(d))
+        send(block_message(B_A, d), pack_a.at[d], xa.at[d, pl.ds(0, cap)], to_a(d))
 
     def a1(d):
-        arrived(f"a{d}")
-        send(f"ay{d}", xa.at[d, pl.ds(0, cap)], xa.at[d, pl.ds(cap, cap)], ydev)
+        arrived(block_message(B_A, d))
+        send(block_message(B_AY, d), xa.at[d, pl.ds(0, cap)], xa.at[d, pl.ds(cap, cap)], ydev)
 
     def a3(d):
-        arrived(f"ay{d}")
+        arrived(block_message(B_AY, d))
 
         def put(at, value):
             ya[d, :, at] = value.astype(bf16)
 
         gated_product(xa[d], gate_v, up_v, down_v, put)
-        send(f"ry{d}", ya.at[d, pl.ds(cap, cap)], ry.at[d], ydev)
+        send(block_message(B_RY, d), ya.at[d, pl.ds(cap, cap)], ry.at[d], ydev)
 
     def a5(d):
-        arrived(f"ry{d}")
+        arrived(block_message(B_RY, d))
         fa[d] = (ya[d, 0:cap].astype(f32) + ry[d].astype(f32)).astype(bf16)
-        send(f"fa{d}", fa.at[d], ret_a.at[pl.ds(d * cap, cap)], from_a(d))
+        send(block_message(B_FA, d), fa.at[d], ret_a.at[pl.ds(d * cap, cap)], from_a(d))
 
     def bo(d):
         pack(0, base + (q + d) % half, pack_b, d - 1, 0)
-        send(f"bo{d}", pack_b.at[d - 1, pl.ds(0, cap)], xb.at[d, pl.ds(0, cap)], to_b(d))
+        send(block_message(B_BO, d), pack_b.at[d - 1, pl.ds(0, cap)], xb.at[d, pl.ds(0, cap)], to_b(d))
 
     def by(d):
         pack(1, base + (q + d) % half, pack_b, d - 1, cap)
-        send(f"by{d}", pack_b.at[d - 1, pl.ds(cap, cap)], xb.at[d, pl.ds(cap, cap)], to_b(d))
+        send(block_message(B_BY, d), pack_b.at[d - 1, pl.ds(cap, cap)], xb.at[d, pl.ds(cap, cap)], to_b(d))
 
     def b3(d):
         if d:
-            arrived(f"bo{d}")
-            arrived(f"by{d}")
+            arrived(block_message(B_BO, d))
+            arrived(block_message(B_BY, d))
         else:
             pack(0, e, xb, 0, 0)
             pack(1, e, xb, 0, cap)
@@ -611,7 +637,7 @@
 
         gated_product(xb[d], gate_v, up_v, down_v, put)
         if d:
-            send(f"fb{d}", yb.at[d - 1], ret_b.at[:, pl.ds(d * cap, cap)], from_b(d))
+            send(block_message(B_FB, d), yb.at[d - 1], ret_b.at[:, pl.ds(d * cap, cap)], from_b(d))
 
     def chosen_slots(columns, first):
         lanes = lax.broadcasted_iota(jnp.int32, (1, half * cap), 1)
@@ -642,9 +668,9 @@
 
     def dense_out():
         for d in range(1, half):
-            arrived(f"fb{d}")
+            arrived(block_message(B_FB, d))
         dense_rows(1)
-        send("dense", dense_s, dense_r, ydev)
+        send(M_DENSE, dense_s, dense_r, ydev)
         dense_rows(0)
 
     def conv(x_v, halo, ext, taps_ref, n, size):
@@ -678,7 +704,7 @@
     local = {}
 
     def mixer_states():
-        for name in ("halo_h", "halo_w", "halo_r"):
+        for name in (M_HALO_H, M_HALO_W, M_HALO_R):
             arrived(name)
         for n in range(0, chans, 256):
             hval[:, n : n + 256] = conv(heads_v, halo_h, ext_h, htaps_ref, n, 256)
@@ -704,10 +730,10 @@
         weighted = (hval[...] * weights).astype(bf16)
         own_s[...] = jnp.dot(jnp.transpose(write).astype(bf16), weighted, preferred_element_type=f32)
         own_d[...] = spread(cum_t[tok_m - 8 : tok_m], 3)[7:8]
-        local.update(cum=cum, cum_t=cum_t, step=step, affinity=affinity)
+        local[0] = (cum, cum_t, step, affinity)
 
     def mixer_rows_local():
-        cum, cum_t, step, affinity = (local[k] for k in ("cum", "cum_t", "step", "affinity"))
+        cum, cum_t, step, affinity = local[0]
         grow_v[...] = spread(jnp.exp(cum_t), 2)
         causal = row >= lane
         for pair in range(heads // 2):
@@ -737,19 +763,19 @@
             out_s[0] = own_s[...].astype(bf16)
             out_d[0] = own_d[...]
 
-        send_if("pair_s", out_s.at[0], in_s.at[0], beside, is_tail)
-        send_if("pair_d", out_d.at[0], in_d.at[0], beside, is_tail)
+        send_if(M_PAIR_S, out_s.at[0], in_s.at[0], beside, is_tail)
+        send_if(M_PAIR_D, out_d.at[0], in_d.at[0], beside, is_tail)
 
     def states_plane():
-        prepare("plane_s", out_s.at[1], in_s.at[1], above)
-        prepare("plane_d", out_d.at[1], in_d.at[1], above)
-        guarded.append(("plane_s", is_head & (plane < planes - 1)))
-        guarded.append(("plane_d", is_head & (plane < planes - 1)))
+        prepare(M_PLANE_S, out_s.at[1], in_s.at[1], above)
+        prepare(M_PLANE_D, out_d.at[1], in_d.at[1], above)
+        guarded.append((M_PLANE_S, is_head & (plane < planes - 1)))
+        guarded.append((M_PLANE_D, is_head & (plane < planes - 1)))
 
         @pl.when(is_head)
         def _():
-            arrived("pair_s")
-            arrived("pair_d")
+            arrived(M_PAIR_S)
+            arrived(M_PAIR_D)
 
         @pl.when(later_head)
         def _():
@@ -769,19 +795,19 @@
             in_d[1] = jnp.zeros(in_d.shape[1:], f32)
             out_s[1] = plane_s[...].astype(bf16)
             out_d[1] = plane_d[...]
-            copies["plane_s"].start()
-            copies["plane_d"].start()
+            copies[M_PLANE_S].start()
+            copies[M_PLANE_D].start()
 
     def states_up(k):
         @pl.when(is_head & (plane == k))
         def _():
-            arrived("plane_s")
-            arrived("plane_d")
+            arrived(M_PLANE_S)
+            arrived(M_PLANE_D)
             if k < planes - 1:
                 out_s[1] = (plane_s[...] + jnp.exp(plane_d[...]) * in_s[1].astype(f32)).astype(bf16)
                 out_d[1] = plane_d[...] + in_d[1]
-                copies["plane_s"].start()
-                copies["plane_d"].start()
+                copies[M_PLANE_S].start()
+                copies[M_PLANE_D].start()
 
     def states_last():
         @pl.when(later_head)
@@ -794,12 +820,12 @@
             bef_s[...] = in_s[1].astype(f32)
             out_s[2] = (own_s[...] + jnp.exp(own_d[...]) * in_s[1].astype(f32)).astype(bf16)
 
-        send_if("last_s", out_s.at[2], in_s.at[2], beside, is_head)
+        send_if(M_LAST_S, out_s.at[2], in_s.at[2], beside, is_head)
 
     def states_in():
         @pl.when(is_tail)
         def _():
-            arrived("last_s")
+            arrived(M_LAST_S)
             bef_s[...] = in_s[2].astype(f32)
 
     def mixer_finish():
@@ -817,51 +843,72 @@
             part = jnp.dot(normed, proj_v[:, n : n + col], preferred_element_type=f32).astype(bf16)
             for i in range(4):
                 mix_v[i, :, n : n + col] = part[i * block : (i + 1) * block]
-        send("mix_core", mix_v.at[t_core], mix_r.at[0], core)
-        send("mix_far", mix_v.at[t_far], mix_r.at[1], core)
+        send(M_MIX_CORE, mix_v.at[t_core], mix_r.at[0], core)
+        send(M_MIX_FAR, mix_v.at[t_far], mix_r.at[1], core)
 
     def mix_across():
-        arrived("mix_core")
-        arrived("mix_far")
+        arrived(M_MIX_CORE)
+        arrived(M_MIX_FAR)
         mix_s[...] = (mix_v[t_y].astype(f32) + mix_r[1].astype(f32)).astype(bf16)
-        send("mix_y", mix_s, mix_ry, ydev)
+        send(M_MIX_Y, mix_s, mix_ry, ydev)
 
     def rows_in():
-        arrived("meta_y")
-        arrived("rows_y")
-
-    steps = {
-        "rows_out": rows_out,
-        "halo_out": halo_out,
-        "weights_out": weights_out,
-        "shared_in": lambda: weights_in(("sgate", "sup", "sdown")),
-        "expert_in": lambda: weights_in(("gate", "up", "down")),
-        "mix_in": lambda: [loads[name].wait() for name in ("ogate", "proj")],
-        "rows_in": rows_in,
-        "states": mixer_states,
-        "local": mixer_rows_local,
-        "pair": states_pair,
-        "plane": states_plane,
-        "last": states_last,
-        "before": states_in,
-        "finish": mixer_finish,
-        "across": mix_across,
-        "dense": dense_out,
-    }
-    numbered = {"a0": a0, "a1": a1, "a3": a3, "a5": a5, "bo": bo, "by": by, "b3": b3, "up": states_up}
-    numbered["shared"] = shared_rows
-    for name in order.split():
-        if name in steps:
-            steps[name]()
-        else:
-            stem, number = name.split(":")
-            numbered[stem](int(number))
-
-    arrived("mix_y")
+        arrived(M_META_Y)
+        arrived(M_ROWS_Y)
+
+    halo_out()
+    a0(0)
+    rows_out()
+    bo(1)
+    bo(2)
+    bo(3)
+    mixer_states()
+    weights_out()
+    states_pair()
+    a0(1)
+    states_plane()
+    mixer_rows_local()
+    a0(2)
+    a1(0)
+    rows_in()
+    by(1)
+    by(2)
+    states_up(1)
+    a1(1)
+    by(3)
+    shared_in()
+    shared_rows(0)
+    shared_rows(1)
+    a0(3)
+    expert_in()
+    b3(0)
+    a3(0)
+    states_up(2)
+    b3(1)
+    b3(2)
+    a5(0)
+    a3(1)
+    a1(2)
+    states_up(3)
+    states_last()
+    a3(2)
+    a1(3)
+    a5(1)
+    b3(3)
+    states_in()
+    mix_in()
+    mixer_finish()
+    a5(2)
+    a3(3)
+    mix_across()
+    a5(3)
+    dense_out()
+
+    arrived(M_MIX_Y)
     mix_out[...] = (mix_v[t].astype(f32) + mix_r[0].astype(f32) + mix_ry[...].astype(f32)).astype(bf16)
     for d in range(half):
-        arrived(f"fa{d}")
-    arrived("dense")
+        arrived(block_message(B_FA, d))
+    arrived(M_DENSE)
     columns = jnp.transpose(meta_v[0])
     picks = chosen_slots(columns, other)
     for n in range(0, width, col):
@@ -880,32 +927,26 @@
             copies[name].wait_send()
 
 
-def exchange_order(half):
-    before = ["rows_out", "halo_out", "a0:0"]
-    before += [f"bo:{d}" for d in range(1, half)]
-    before += ["weights_out", "states", "pair"]
-    if half > 1:
-        before += ["a0:1"]
-    before += ["plane", "local", "up:1"]
-    before += [f"a0:{d}" for d in range(2, half)]
-    after = {0: ["rows_in"] + [f"by:{d}" for d in range(1, half)]}
-    after[0] += ["shared_in", "shared:1", "shared:0", "expert_in", "b3:0"]
-    after.setdefault(1, []).extend(["up:2"])
-    for d in range(1, half):
-        after.setdefault(d, []).append(f"b3:{d}")
-    for k in range(3, half):
-        after.setdefault(k - 1, []).append(f"up:{k}")
-    after.setdefault(half - 2, []).append("last")
-    after.setdefault(half - 1, []).extend(["before", "mix_in", "finish"])
-    after[half] = ["across"]
-    after[half + 1] = ["dense"]
-    steps = list(before)
-    for at in range(half + 2):
-        for kind, lag in (("a5", 2), ("a3", 1), ("a1", 0)):
-            if 0 <= at - lag < half:
-                steps.append(f"{kind}:{at - lag}")
-        steps += after.get(at, [])
-    return " ".join(steps)
+def settle_kernel(mix_ref, moe_ref, mix_out, moe_out, sem):
+    copies = [
+        pltpu.make_async_copy(mix_ref, mix_out, sem.at[0]),
+        pltpu.make_async_copy(moe_ref, moe_out, sem.at[1]),
+    ]
+    for copy in copies:
+        copy.start()
+    for copy in copies:
+        copy.wait()
+
+
+def settle(mix, moe):
+    return pl.pallas_call(
+        settle_kernel,
+        out_shape=tuple(jax.ShapeDtypeStruct(x.shape, x.dtype) for x in (mix, moe)),
+        in_specs=[pl.BlockSpec(memory_space=pltpu.VMEM)] * 2,
+        out_specs=tuple([pl.BlockSpec(memory_space=pl.ANY)] * 2),
+        scratch_shapes=[pltpu.SemaphoreType.DMA((2,))],
+        name="settle",
+    )(mix, moe)
 
 
 def exchange(ep_count, capacity, small, large):
@@ -917,7 +958,7 @@
     tok_m, chans = heads.shape
     state = write.shape[1]
     mix_block = tok_m // 4
-    count = len(message_names(half))
+    count = SINGLE + BLOCK_KINDS * half
     shapes = [(array.shape, bf16) for array in (rows, heads, write, read, ogate, proj)]
     shapes += [((2, *array.shape), bf16) for array in (gate, up, down, sgate, sup, sdown)]
     shapes += [
@@ -963,7 +1004,7 @@
     any_spec = pl.BlockSpec(memory_space=pl.ANY)
     vmem_spec = pl.BlockSpec(memory_space=pltpu.VMEM)
     return pl.pallas_call(
-        functools.partial(exchange_kernel, ep_count, capacity, exchange_order(half)),
+        functools.partial(exchange_kernel, ep_count, capacity),
         out_shape=(
             jax.ShapeDtypeStruct((mix_block, width), bf16),
             jax.ShapeDtypeStruct((tok, width), bf16),
@@ -1035,7 +1076,7 @@
         shared_up_weight,
         shared_down_weight,
     )
-    return exchange(ep_count, capacity, small, large)
+    return settle(*exchange(ep_count, capacity, small, large))
 
 
 def fits_direct(mesh, rows, mix_rows, top_count, experts, groups):
@@ -1046,7 +1087,7 @@
         tp_count == 4
         and groups == tp_count
         and experts == ep_count
-        and ep_count in (4, 8)
+        and ep_count == 8
         and top_count == 2
         and capacity % 16 == 0
         and tok_local == 128

time: 96.9 us -> 91.7 us (0.946)
  the two profiles are of different devices: /device:TPU:24 before, /device:TPU:8 now
where the time goes in v4:
time: 91.7 us; the launch traced here: 91.5 us
  Pallas kernels  90.7 us (99%)
    pallas_call x1, Pallas kernels, exchange(): pl.pallas_call(functools.partial(exchange_kernel, ep_count, capacity), ou...  88.7 us
    pallas_call x1, Pallas kernels, settle(): pl.pallas_call(settle_kernel, out_shape=tuple((jax.ShapeDtypeStruct(x.sha...  1.97 us

profile of v4, /device:TPU:8, one launch (start us, length us, event | category | flops | bytes accessed | tf_op | source)
XLA Modules:
  0.0 91.5 jit_solution(2721098984142458223)
XLA Ops:
  0.6 88.7 %mixer_and_experts.1 = (bf16[32,2048]{1,0:T(8,128)(2,1)}, bf16[128,2048]{1,0:T(8,128)(2,1)}) custom-call(bf16[128,2048]{1,0:T(8,128)(2,1)} %rows_hbm.1, bf16[128,1024]{1,0:T(8,128)(2,1)} %heads_hbm.1, bf16[128,128]{1,0:T(8,128)(2,1)} %write_hbm.1, bf16[128,128]{1,0:T(8,128)(2,1)} %read_hbm.1, bf16[128,1024]{1,0:T(8,128)(2,1)} %ogate_hbm.1, ...), custom_call_target="tpu_custom_call" | custom-call | tf_op jit(solution)/shard_map/mixer_and_experts/pallas_call | solution.py:1006
  89.4 2.0 %settle.1 = (bf16[32,2048]{1,0:T(8,128)(2,1)}, bf16[128,2048]{1,0:T(8,128)(2,1)}) custom-call(bf16[32,2048]{1,0:T(8,128)(2,1)} %get-tuple-element.4.mix_ref, bf16[128,2048]{1,0:T(8,128)(2,1)} %get-tuple-element.5.moe_ref), custom_call_target="tpu_custom_call" | custom-call | tf_op jit(solution)/shard_map/settle/pallas_call | solution.py:942

commit v5 on v4

--- a/solution.py
+++ b/solution.py
@@ -376,6 +376,9 @@
     ext_w,
     ext_r,
     hval,
+    write_f,
+    read_f,
+    weights_f,
     y_v,
     read_b,
     grow_v,
@@ -521,7 +524,6 @@
         return carry
 
     lax.fori_loop(0, tok // 16, norm_rows, 0)
-    pl.semaphore_wait(barrier, len(peers))
 
     def pack(pos, expert_at, ref, lead, low):
         places = lax.broadcasted_iota(jnp.int32, (cap, tok), 0) + expert_at * cap
@@ -673,20 +675,29 @@
         send(M_DENSE, dense_s, dense_r, ydev)
         dense_rows(0)
 
-    def conv(x_v, halo, ext, taps_ref, n, size):
-        at = slice(n, n + size)
+    def taps_sum(ext, taps_ref, at, length):
         taps = taps_ref.shape[0]
         edge = ext.shape[0] - tok_m
-        first = halo.shape[0] - edge
-        there = jnp.where(e > 0, 1.0, 0.0).astype(f32)
-        ext[0:edge, at] = halo[first:, at].astype(f32) * there
-        ext[edge:, at] = x_v[:, at].astype(f32)
         total = None
         for j in range(taps):
             low = edge - taps + 1 + j
-            part = taps_ref[j : j + 1, at].astype(f32) * ext[low : low + tok_m, at]
+            part = taps_ref[j : j + 1, at].astype(f32) * ext[low : low + length, at]
             total = part if total is None else total + part
         return jax.nn.silu(total)
+
+    def conv(x_v, ext, taps_ref, n, size):
+        at = slice(n, n + size)
+        edge = ext.shape[0] - tok_m
+        ext[0:edge, at] = jnp.zeros((edge, size), f32)
+        ext[edge:, at] = x_v[:, at].astype(f32)
+        return taps_sum(ext, taps_ref, at, tok_m)
+
+    def conv_first(halo, ext, taps_ref, n, size):
+        at = slice(n, n + size)
+        edge = ext.shape[0] - tok_m
+        there = jnp.where(e > 0, 1.0, 0.0).astype(f32)
+        ext[0:edge, at] = halo[halo.shape[0] - edge :, at].astype(f32) * there
+        return taps_sum(ext, taps_ref, at, edge)
 
     head_row = lax.broadcasted_iota(jnp.int32, (heads, chans), 0)
     lane_head = lax.broadcasted_iota(jnp.int32, (heads, chans), 1) - head_row * head_dim
@@ -703,15 +714,12 @@
 
     local = {}
 
-    def mixer_states():
-        for name in (M_HALO_H, M_HALO_W, M_HALO_R):
-            arrived(name)
+    def mixer_early():
         for n in range(0, chans, 256):
-            hval[:, n : n + 256] = conv(heads_v, halo_h, ext_h, htaps_ref, n, 256)
+            hval[:, n : n + 256] = conv(heads_v, ext_h, htaps_ref, n, 256)
         states = write_v.shape[1]
-        write = conv(write_v, halo_w, ext_w, wtaps_ref, 0, states)
-        read = conv(read_v, halo_r, ext_r, rtaps_ref, 0, states)
-        read_b[...] = read.astype(bf16)
+        write_f[...] = conv(write_v, ext_w, wtaps_ref, 0, states)
+        read_f[...] = conv(read_v, ext_r, rtaps_ref, 0, states)
         step = jax.nn.softplus(step_ref[...])
         square_row = lax.broadcasted_iota(jnp.int32, (heads, heads), 0)
         square_lane = lax.broadcasted_iota(jnp.int32, (heads, heads), 1)
@@ -723,18 +731,35 @@
         cum = jnp.dot(rate, upto, precision=highest, preferred_element_type=f32)
         cum_t = jnp.transpose(cum)
         to_end = jnp.exp(cum[:, tok_m - 1 : tok_m] - cum) * step
+        weights_f[...] = spread(jnp.transpose(to_end), 2)
+        own_d[...] = spread(cum_t[tok_m - 8 : tok_m], 3)[7:8]
+        grow_v[...] = spread(jnp.exp(cum_t), 2)
+        local[0] = (cum, cum_t, step)
+
+    def mixer_states():
+        for name in (M_HALO_H, M_HALO_W, M_HALO_R):
+            arrived(name)
+        edge = ext_h.shape[0] - tok_m
+        for n in range(0, chans, 256):
+            hval[0:edge, n : n + 256] = conv_first(halo_h, ext_h, htaps_ref, n, 256)
+        states = write_v.shape[1]
+        write_f[0:edge, :] = conv_first(halo_w, ext_w, wtaps_ref, 0, states)
+        read_f[0:edge, :] = conv_first(halo_r, ext_r, rtaps_ref, 0, states)
+        weighted = (hval[...] * weights_f[...]).astype(bf16)
+        own_s[...] = jnp.dot(
+            jnp.transpose(write_f[...]).astype(bf16), weighted, preferred_element_type=f32
+        )
+
+    def mixer_rows_local():
+        cum, cum_t, step = local[0]
+        read_b[...] = read_f[...].astype(bf16)
         affinity = lax.dot_general(
-            read, write, (((1,), (1,)), ((), ())), precision=highest, preferred_element_type=f32
+            read_f[...],
+            write_f[...],
+            (((1,), (1,)), ((), ())),
+            precision=highest,
+            preferred_element_type=f32,
         )
-        weights = spread(jnp.transpose(to_end), 2)
-        weighted = (hval[...] * weights).astype(bf16)
-        own_s[...] = jnp.dot(jnp.transpose(write).astype(bf16), weighted, preferred_element_type=f32)
-        own_d[...] = spread(cum_t[tok_m - 8 : tok_m], 3)[7:8]
-        local[0] = (cum, cum_t, step, affinity)
-
-    def mixer_rows_local():
-        cum, cum_t, step, affinity = local[0]
-        grow_v[...] = spread(jnp.exp(cum_t), 2)
         causal = row >= lane
         for pair in range(heads // 2):
             at = slice(pair * 2 * head_dim, (pair + 1) * 2 * head_dim)
@@ -856,14 +881,16 @@
         arrived(M_META_Y)
         arrived(M_ROWS_Y)
 
+    pl.semaphore_wait(barrier, len(peers))
     halo_out()
     a0(0)
     rows_out()
     bo(1)
     bo(2)
     bo(3)
+    weights_out()
+    mixer_early()
     mixer_states()
-    weights_out()
     states_pair()
     a0(1)
     states_plane()
@@ -968,6 +995,9 @@
         ((tok_m + 8, chans), f32),
         ((tok_m + 8, state), f32),
         ((tok_m + 8, state), f32),
+        ((tok_m, chans), f32),
+        ((tok_m, state), f32),
+        ((tok_m, state), f32),
         ((tok_m, chans), f32),
         ((tok_m, chans), f32),
         ((tok_m, state), bf16),

time: 91.7 us -> 89 us (0.971)
  the two profiles are of different devices: /device:TPU:8 before, /device:TPU:0 now
where the time goes in v5:
time: 89 us; the launch traced here: 88.7 us
  Pallas kernels  87.9 us (99%)
    pallas_call x1, Pallas kernels, exchange(): pl.pallas_call(functools.partial(exchange_kernel, ep_count, capacity), ou...  85.9 us
    pallas_call x1, Pallas kernels, settle(): pl.pallas_call(settle_kernel, out_shape=tuple((jax.ShapeDtypeStruct(x.sha...  1.97 us

profile of v5, /device:TPU:0, one launch (start us, length us, event | category | flops | bytes accessed | tf_op | source)
XLA Modules:
  0.0 88.7 jit_solution(11462025700247581596)
XLA Ops:
  0.6 85.9 %mixer_and_experts.1 = (bf16[32,2048]{1,0:T(8,128)(2,1)}, bf16[128,2048]{1,0:T(8,128)(2,1)}) custom-call(bf16[128,2048]{1,0:T(8,128)(2,1)} %rows_hbm.1, bf16[128,1024]{1,0:T(8,128)(2,1)} %heads_hbm.1, bf16[128,128]{1,0:T(8,128)(2,1)} %write_hbm.1, bf16[128,128]{1,0:T(8,128)(2,1)} %read_hbm.1, bf16[128,1024]{1,0:T(8,128)(2,1)} %ogate_hbm.1, ...), custom_call_target="tpu_custom_call" | custom-call | tf_op jit(solution)/shard_map/mixer_and_experts/pallas_call | solution.py:1036
  86.6 2.0 %settle.1 = (bf16[32,2048]{1,0:T(8,128)(2,1)}, bf16[128,2048]{1,0:T(8,128)(2,1)}) custom-call(bf16[32,2048]{1,0:T(8,128)(2,1)} %get-tuple-element.4.mix_ref, bf16[128,2048]{1,0:T(8,128)(2,1)} %get-tuple-element.5.moe_ref), custom_call_target="tpu_custom_call" | custom-call | tf_op jit(solution)/shard_map/settle/pallas_call | solution.py:969
